TPU v7x, 256 devices: a whole 4x4x8 slice. The times are simulated.
256 devices in a mesh: sp: 128 (over z, y, x), tp: 2 (over core).
Axes of the slice: x: 4, y: 4, z: 8, core: 2. Of those that a mesh axis runs over, the one named last changes fastest.
Arguments:
- queries: bfloat16 [196608, 1024], P('sp', 'tp'), may hold values from -6 to 6
- forget_logit: bfloat16 [196608, 1024], P('sp', 'tp'), may hold values from -8 to 8
- value_rows: bfloat16 [196608, 1024], P('sp', 'tp'), may hold values from -10 to 10
- out_gate: bfloat16 [196608, 1024], P('sp', 'tp'), may hold values from -6 to 6
- floor_gap: float32 [1024], P('tp'), may hold values from 0 to 0.1, as said below
- head_gain: float32 [1024], P('tp'), may hold values from 0.1 to 1.9
- state_in: float32 [8, 128, 128], P('tp'), may hold values from -0.625 to 0.625
- out_weight: bfloat16 [1024, 2048], P('tp'), may hold values from -0.1875 to 0.1875
Outputs:
- projected: bfloat16 [196608, 2048], P(('sp', 'tp'))
- state_out: float32 [8, 16384], P('tp', 'sp')
Inputs may be any that keep to these rules, and one draw needn't show every extreme that they name: `floor_gap`: strictly between 0 and 0.1.
All inputs are finite; a program needn't handle non-finite values.
Results may differ from a plain program's by a relative error of at most 0.009.
Values may be sent and summed in bfloat16 or wider, within the bound.
No kernel may reach another device: no remote copies, remote signals or barrier semaphores. Data moves between devices by JAX's collectives and lax.ppermute only.
A program may use at most 128 MiB of HBM per device.

v0:
```python
import jax
import jax.numpy as jnp
from jax import lax
from jax.sharding import Mesh
from jax.sharding import PartitionSpec as P

BLOCK = 128
SP = ("sp_0", "sp_1", "sp_2")
SP_TP = ("sp_0", "sp_1", "sp_2", "tp")


epsilon = 1e-06


def neutral_like(value, identity):
    return jax.tree.map(
        lambda a, e: jnp.broadcast_to(jnp.asarray(e, a.dtype), a.shape), value, identity
    )


def entering(value, axes, combine, identity):
    before = start = neutral_like(value, identity)
    so_far = value
    for axis in reversed(axes):
        length, mine = (lax.axis_size(axis), lax.axis_index(axis))
        pieces = jax.tree.map(lambda part: lax.all_gather(part, axis), so_far)
        inside, so_far = (start, start)
        for k in range(length):
            passed = k < mine
            so_far = combine(so_far, jax.tree.map(lambda part: part[k], pieces))
            inside = jax.tree.map(lambda new, old: jnp.where(passed, new, old), so_far, inside)
        before = combine(inside, before)
    return before


def broadcast_by_axis(value, axes, root):
    value = jnp.where(lax.axis_index(axes) == root, value, jnp.zeros_like(value))
    for axis in axes:
        value = lax.psum(value, axis)
    return value


def to_blocks(values, head_count):
    blocks = values.shape[0] // BLOCK
    return values.reshape(blocks, BLOCK, head_count, values.shape[1] // head_count)


def join_state(earlier, later):
    return (earlier[0] * later[0], later[0][..., None] * earlier[1] + later[1])


def per_device(
    queries, forget_logit, value_rows, out_gate, floor_gap, head_gain, state_in, out_weight
):
    span_rows = queries.shape[0]
    head_count = state_in.shape[0]
    key_gate = to_blocks(floor_gap * jax.nn.sigmoid(-forget_logit.astype(jnp.float32)), head_count)
    log_forget = jnp.log1p(-key_gate)
    reader = to_blocks(jax.nn.silu(queries.astype(jnp.float32)), head_count)
    written_update = to_blocks(value_rows.astype(jnp.float32), head_count)
    positions = jnp.arange(BLOCK)
    causal = positions[:, None] >= positions[None, :]
    lower_ones = causal.astype(jnp.float32)
    cumul = jnp.einsum("cs,nshk->nchk", lower_ones, log_forget)
    scaled_readout = reader * jnp.exp(cumul)
    key_scaled = key_gate * jnp.exp(-cumul)
    scores = jnp.einsum("nchk,nshk->nhcs", scaled_readout, key_scaled)
    scores = jnp.where(causal, scores, 0.0)
    within = jnp.einsum("nhcs,nshv->nchv", scores, written_update)
    block_log_decay = cumul[:, -1]
    decay_to_finish = key_gate * jnp.exp(block_log_decay[:, None] - cumul)
    segment_state = jnp.einsum("nshk,nshv->nhkv", decay_to_finish, written_update)
    block_final_rows = jnp.cumsum(block_log_decay, axis=0)
    starts = block_final_rows - block_log_decay
    overall_log_decay = block_final_rows[-1]
    block_ids = jnp.arange(block_final_rows.shape[0])
    earlier_mask = (block_ids[:, None] > block_ids[None, :])[:, :, None, None]
    spacing = jnp.where(earlier_mask, starts[:, None] - block_final_rows[None, :], 0.0)
    carry_weight = jnp.where(earlier_mask, jnp.exp(spacing), 0.0)
    local_before = jnp.einsum("jihk,ihkv->jhkv", carry_weight, segment_state)
    decay_dev = jnp.exp(overall_log_decay)
    state_dev = jnp.einsum(
        "lpt,lptr->ptr", jnp.exp(overall_log_decay[None] - block_final_rows), segment_state
    )
    prefix_decay, prefix_state = entering(
        (decay_dev, state_dev),
        SP,
        join_state,
        (jnp.ones_like(decay_dev), jnp.zeros_like(state_dev)),
    )
    incoming = prefix_decay[..., None] * state_in + prefix_state
    before = local_before + jnp.exp(starts)[..., None] * incoming[None]
    unscaled_output = within + jnp.einsum("nchk,nhkv->nchv", scaled_readout, before)
    mean_square = jnp.mean(unscaled_output * unscaled_output, axis=-1, keepdims=True)
    gain_rows = head_gain.reshape(head_count, -1)
    normed = unscaled_output * lax.rsqrt(mean_square + epsilon) * gain_rows
    gating = jax.nn.silu(to_blocks(out_gate.astype(jnp.float32), head_count))
    gated = (normed * gating).astype(jnp.bfloat16).reshape(span_rows, -1)
    regrouped = lax.all_to_all(gated, "tp", split_axis=0, concat_axis=1, tiled=True)
    summed = jnp.dot(
        regrouped,
        lax.all_gather(out_weight, "tp", axis=0, tiled=True),
        preferred_element_type=jnp.float32,
    )
    projected = summed.astype(jnp.bfloat16)
    finished = (decay_dev[..., None] * incoming + state_dev).reshape(head_count, -1)
    whole_final = broadcast_by_axis(
        finished.astype(jnp.bfloat16), SP, lax.axis_size(SP) - 1
    ).astype(finished.dtype)
    share = whole_final.shape[1] // lax.axis_size(SP)
    offset = lax.axis_index(SP) * share
    state_out = lax.dynamic_slice_in_dim(whole_final, offset, share, 1)
    return (projected, state_out)


def solution(mesh):
    torus = Mesh(mesh.devices.reshape(8, 4, 4, mesh.shape["tp"]), ("sp_0", "sp_1", "sp_2", "tp"))
    placed = (
        P(SP, "tp"),
        P(SP, "tp"),
        P(SP, "tp"),
        P(SP, "tp"),
        P("tp"),
        P("tp"),
        P("tp", None, None),
        P("tp", None),
    )
    return jax.shard_map(
        per_device,
        mesh=torus,
        in_specs=placed,
        out_specs=(P(SP_TP, None), P("tp", SP)),
        check_vma=False,
    )
```

profile of v0, /device:TPU:1, one launch (start us, length us, event | category | flops | bytes accessed | tf_op | source)
XLA Modules:
  0.0 313.0 jit_solution(17621082454385104322)
XLA Ops:
  8.0 0.0 all-gather.12.cloned.1.call-start
  8.0 3.9 %divide_multiply_fusion = f32[1536,512]{1,0:T(8,128)} fusion(bf16[1536,512]{1,0:T(8,128)(2,1)} %param.9, f32[512]{0:T(512)} %param.12), kind=kLoop, calls=%fused_computation.34 | loop fusion | flops 3145728 | bytes 4720640 | tf_op jit(solution)/shard_map/mul | solution.py:57
  11.9 3.1 %reshape.230 = f32[12,128,4,128]{3,2,1,0:T(4,128)S(1)} reshape(f32[1536,512]{1,0:T(8,128)} %divide_multiply_fusion) | data formatting | bytes 6291456 | tf_op jit(solution)/shard_map/reshape | solution.py:45
  15.1 1.7 copy-done
  16.8 2.3 negate_log-plus-one_fusion
  19.0 0.6 fusion.31
  19.7 0.2 copy.44
  19.9 3.5 %reshape.231 = bf16[12,128,4,128]{3,2,1,0:T(4,128)(2,1)} reshape(bf16[1536,512]{1,0:T(8,128)(2,1)} %param.10) | data formatting | bytes 3145728 | tf_op jit(solution)/shard_map/reshape | solution.py:45
  23.4 3.3 %fusion.15 = bf16[12,4,128,128]{3,2,1,0:T(8,128)(2,1)S(1)} fusion(f32[12,128,4,128]{3,1,2,0:T(8,128)S(1)} %fusion.31, f32[12,128,4,128]{3,2,1,0:T(4,128)} %copy-done, f32[12,4,128]{2,1,0:T(4,128)S(1)} %bitcast.247, bf16[12,128,4,128]{3,2,1,0:T(4,128)(2,1)} %reshape.231), kind=kOutput, calls=%fused_computation.23 | convolution fusion | flops 202899456 | bytes 9461760 | tf_op jit(solution)/shard_map/nshk,nshv->nhkv/dot_general | solution.py:72
  26.7 1.1 copy-done.2
  27.8 1.9 fusion
  29.8 0.0 all-gather.6.cloned.1.call-start
  29.8 9.3 %all_gather.29 = f32[4,4,128]{2,1,0:T(4,128)S(1)} all-gather(f32[1,4,128]{2,1,0:T(4,128)S(1)} %get-tuple-element.7), channel_id=1, replica_groups=mesh['sp_0'=8,'sp_1'=4,'sp_2'=4,'tp'=2] {'sp_2'}, dimensions={0}, use_global_device_ids=true | all-gather | bytes 10240 | tf_op jit(solution)/shard_map/all_gather | solution.py:26
  39.1 19.1 %all-gather.12.cloned.1.call-done = f32[16,128,128]{2,1,0:T(8,128)} async-done(((f32[4,128,128]{2,1,0:T(8,128)}), f32[16,128,128]{2,1,0:T(8,128)}) %all-gather.12.cloned.1.call-update) | async-done | bytes 1048592 | tf_op jit(solution)/shard_map/all_gather | solution.py:26
  58.3 2.2 bitcast_add_fusion.6
  60.5 0.0 all-gather.8.cloned.1.call-start
  60.6 8.5 %all_gather.30 = f32[4,4,128]{2,1,0:T(4,128)S(1)} all-gather(f32[1,4,128]{2,1,0:T(4,128)S(1)} %get-tuple-element.20), channel_id=1, replica_groups=mesh['sp_0'=8,'sp_1'=4,'sp_2'=4,'tp'=2] {'sp_1'}, dimensions={0}, use_global_device_ids=true | all-gather | bytes 10240 | tf_op jit(solution)/shard_map/all_gather | solution.py:26
  69.0 18.7 %all-gather.6.cloned.1.call-done = f32[4,4,128,128]{3,2,1,0:T(8,128)} async-done(((f32[1,4,128,128]{3,2,1,0:T(8,128)}), f32[4,4,128,128]{3,2,1,0:T(8,128)}) %all-gather.6.cloned.1.call-update) | async-done | bytes 1048592 | tf_op jit(solution)/shard_map/all_gather | solution.py:26
  87.7 2.2 multiply_add_fusion
  90.0 0.0 all-reduce.4.cloned.1.call-start
  90.1 18.7 %all_gather.31 = f32[8,4,128]{2,1,0:T(4,128)S(1)} all-gather(f32[1,4,128]{2,1,0:T(4,128)S(1)} %get-tuple-element.16), channel_id=1, replica_groups=mesh['sp_0'=8,'sp_1'=4,'sp_2'=4,'tp'=2] {'sp_0'}, dimensions={0}, use_global_device_ids=true | all-gather | bytes 18432 | tf_op jit(solution)/shard_map/all_gather | solution.py:26
  108.9 20.3 %all-gather.8.cloned.1.call-done = f32[8,4,128,128]{3,2,1,0:T(8,128)} async-done(((f32[1,4,128,128]{3,2,1,0:T(8,128)}), f32[8,4,128,128]{3,2,1,0:T(8,128)}) %all-gather.8.cloned.1.call-update) | async-done | bytes 2097168 | tf_op jit(solution)/shard_map/all_gather | solution.py:26
  129.2 4.6 %fusion.68 = (bf16[1,4,128,128]{3,2,1,0:T(8,128)(2,1)S(1)}, f32[4,128,128]{2,1,0:T(8,128)}) fusion(f32[4,128,128]{2,1,0:T(8,128)S(1)} %bitcast.242, f32[4,128]{1,0:T(4,128)S(1)} %fusion.80, pred[]{:T(512)S(6)} %eq.3, pred[]{:T(512)S(6)} %gt.89, pred[]{:T(512)S(6)} %gt.88, pred[]{:T(512)S(6)} %gt.87, f32[16,128,128]{2,1,0:T(8,128)} %all-gather.12.cloned.1.call-done, ...), kind=kLoop, calls=%fused_computation.84 | loop fusion | flops 3604480 | bytes 5152785
  133.8 0.8 copy.89
  134.6 0.0 all-reduce.6.cloned.1.call-start
  134.7 70.4 %all-reduce.4.cloned.1.call-done = bf16[4,16384]{1,0:T(4,128)(2,1)} async-done(((bf16[4,16384]{1,0:T(4,128)(2,1)}), bf16[4,16384]{1,0:T(4,128)(2,1)}) %all-reduce.4.cloned.1.call-update) | async-done | bytes 131088 | tf_op jit(solution)/shard_map/psum | solution.py:39
  205.1 0.0 all-gather.10.cloned.1.call-start
  205.1 0.5 all-gather.10.cloned.1.call-update
  205.6 0.2 all-reduce.8.cloned.1.call-start
  205.9 0.1 copy.34
  206.0 0.8 copy.36
  206.9 0.8 copy.33
  207.8 3.9 %convert_multiply_fusion = f32[1536,512]{1,0:T(8,128)} fusion(bf16[1536,512]{1,0:T(8,128)(2,1)} %param.8), kind=kLoop, calls=%fused_computation.9 | loop fusion | flops 3932160 | bytes 4718592 | tf_op jit(solution)/shard_map/jit(silu)/mul | solution.py:59
  211.7 4.9 %reshape.229 = f32[12,128,4,128]{3,2,1,0:T(4,128)} reshape(f32[1536,512]{1,0:T(8,128)} %convert_multiply_fusion) | data formatting | bytes 6291456 | tf_op jit(solution)/shard_map/reshape | solution.py:45
  216.6 4.1 %reshape.235 = f32[12,128,4,128]{3,2,1,0:T(4,128)} reshape(bf16[1536,512]{1,0:T(8,128)(2,1)} %param.11) | data formatting | bytes 4718592 | tf_op jit(solution)/shard_map/reshape | solution.py:45
  220.7 5.0 %copy.39 = f32[12,128,4,128]{1,3,2,0:T(8,128)} copy(f32[12,128,4,128]{3,2,1,0:T(4,128)} %reshape.235) | data formatting | bytes 6291456 | tf_op jit(solution)/shard_map/reshape | solution.py:45
  225.6 4.5 %bitcast_add_fusion = bf16[12,4,128,128]{3,0,2,1:T(8,128)(2,1)S(1)} fusion(f32[4,128,128]{2,1,0:T(8,128)} %get-tuple-element.3, f32[12,4,128]{0,2,1:T(8,128)} %copy.36, f32[12,4,128]{0,2,1:T(8,128)S(1)} %copy.34, f32[12,4,128]{0,2,1:T(8,128)} %copy.33, pred[12,12]{1,0:T(8,128)(4,1)S(1)} %iota_compare_fusion.2, bf16[12,4,128,128]{3,2,1,0:T(8,128)(2,1)} %copy-done.2), kind=kOutput, calls=%fused_computation.4 | convolution fusion | flops 21454848 | bytes 3481744 | tf_op jit(solution)/shard_map/jihk,ihkv->jhkv/dot_general | solution.py:80
  230.1 2.9 fusion.11
  233.0 8.2 %multiply_reduce_fusion = (f32[12,128,4]{1,2,0:T(4,128)S(1)}, f32[12,128,4,128]{1,3,2,0:T(8,128)}) fusion(f32[12,4,128,128]{3,2,1,0:T(8,128)} %fusion.11, bf16[12,128,4,128]{3,2,1,0:T(4,128)(2,1)} %reshape.231, pred[128,128]{1,0:T(8,128)(4,1)S(1)} %iota_compare_fusion, f32[12,128,4,128]{3,1,2,0:T(8,128)S(1)} %fusion.31, f32[12,128,4,128]{3,2,1,0:T(4,128)} %copy-done, ...), kind=kOutput, calls=%fused_computation.22 | convolution fusion | flops 408152064 | bytes 17342464 | tf_op jit(solution)/shard_map/nhcs,nshv->nchv/dot_general | solution.py:69
  241.3 3.9 %multiply_convert_fusion = bf16[12,128,4,128]{1,3,2,0:T(8,128)(2,1)S(1)} fusion(f32[12,128,4,128]{1,3,2,0:T(8,128)} %copy.39, f32[12,128,4,128]{1,3,2,0:T(8,128)} %get-tuple-element.25, f32[4,128]{1,0:T(4,128)S(1)} %bitcast.251, f32[12,128,4]{1,2,0:T(4,128)S(1)} %add_rsqrt_fusion), kind=kLoop, calls=%fused_computation.21 | loop fusion | flops 6291456 | bytes 7890944 | tf_op jit(solution)/shard_map/convert_element_type | solution.py:98
  245.2 1.1 copy.40
  246.2 0.6 all_to_all.14
  246.9 10.4 %all_to_all.19 = bf16[2,768,512]{2,1,0:T(8,128)(2,1)S(1)} all-to-all(bf16[2,768,512]{2,1,0:T(8,128)(2,1)S(1)} %all_to_all.14), channel_id=1, replica_groups=mesh['sp_0'=8,'sp_1'=4,'sp_2'=4,'tp'=2] {'tp'}, dimensions={0} | all-to-all | bytes 3145728 | tf_op jit(solution)/shard_map/all_to_all | solution.py:99
  257.3 0.7 copy.41
  258.1 0.0 all-gather.10.cloned.1.call-done
  258.1 7.0 %convolution_convert_fusion = bf16[768,2048]{1,0:T(8,128)(2,1)} fusion(bf16[768,1024]{0,1:T(8,128)(2,1)S(1)} %bitcast.240, bf16[1024,2048]{1,0:T(8,128)(2,1)} %all-gather.10.cloned.1.call-done), kind=kOutput, calls=%fused_computation.11 | convolution fusion | flops 3222798336 | bytes 8912896 | tf_op jit(solution)/shard_map/dot_general | solution.py:100
  265.2 39.2 %all-reduce.8.cloned.1.call-done = bf16[4,16384]{1,0:T(4,128)(2,1)} async-done(((bf16[4,16384]{1,0:T(4,128)(2,1)}), bf16[4,16384]{1,0:T(4,128)(2,1)}) %all-reduce.8.cloned.1.call-update) | async-done | bytes 131088 | tf_op jit(solution)/shard_map/psum | solution.py:39
  304.4 1.2 dynamic-slice_convert_fusion
  (32 shorter events, 0.3 us)
Async XLA Ops:
  8.0 50.3 %all-gather.12.cloned.1.call-start = ((), (), s32[]{:S(2)}) async-start(), calls=%async_computation.7 | async-start | bytes 1310720 | tf_op jit(solution)/shard_map/all_gather | solution.py:26
  15.1 1.7 copy-start
  26.7 1.1 copy-start.2
  29.7 99.5 %copy-start.3 = (f32[4,128,1,128]{3,2,1,0:T(1,128)S(1)}, f32[4,128,1,128]{3,2,1,0:T(1,128)}, u32[]{:S(2)}) copy-start(f32[4,128,1,128]{3,2,1,0:T(1,128)} %fusion) | copy-start | bytes 786436
  29.8 58.0 %all-gather.6.cloned.1.call-start = ((), (), s32[]{:S(2)}) async-start(), calls=%async_computation.1 | async-start | bytes 1310720 | tf_op jit(solution)/shard_map/all_gather | solution.py:26
  60.5 68.7 %all-gather.8.cloned.1.call-start = ((), (), s32[]{:S(2)}) async-start(), calls=%async_computation.2 | async-start | bytes 2359296 | tf_op jit(solution)/shard_map/all_gather | solution.py:26
  90.0 115.1 %all-reduce.4.cloned.1.call-start = ((), (), s32[]{:S(2)}) async-start(), calls=%async_computation.4 | async-start | bytes 262144 | tf_op jit(solution)/shard_map/psum | solution.py:39
  134.6 123.5 %all-reduce.6.cloned.1.call-start = ((), (), s32[]{:S(2)}) async-start(), calls=%async_computation.5 | async-start | bytes 262144 | tf_op jit(solution)/shard_map/psum | solution.py:39
  205.1 53.1 %all-gather.10.cloned.1.call-start = ((), (), s32[]{:S(2)}) async-start(), calls=%async_computation.3 | async-start | bytes 6291456 | tf_op jit(solution)/shard_map/all_gather | solution.py:102
  205.6 98.7 %all-reduce.8.cloned.1.call-start = ((), (), s32[]{:S(2)}) async-start(), calls=%async_computation.6 | async-start | bytes 262144 | tf_op jit(solution)/shard_map/psum | solution.py:39
  225.6 4.5 %copy-start.1 = (f32[12,128,4,128]{3,2,1,0:T(4,128)S(1)}, f32[12,128,4,128]{3,2,1,0:T(4,128)}, u32[]{:S(2)}) copy-start(f32[12,128,4,128]{3,2,1,0:T(4,128)} %reshape.229) | copy-start | bytes 9437188
  233.0 8.2 %copy-start.4 = (f32[512]{0:T(512)S(1)}, f32[512]{0:T(512)}, u32[]{:S(2)}) copy-start(f32[512]{0:T(512)} %param.13) | copy-start | bytes 6148
Sparse Core Ops, SparseCore 0:
  29.9 28.3 all-gather.11
  60.6 27.0 all-gather.5
  90.1 39.0 all-gather.7
  134.7 70.2 all-reduce.3
  207.2 48.0 all-reduce.5
  258.2 46.1 all-reduce.7
Sparse Core Ops, SparseCore 1:
  207.3 23.1 all-gather.9
where the time goes:
time: 315 us; the launch traced here: 313 us
  waiting for transfers between devices  168 us (53%)
  blocking collectives  47 us (15%)
  local copies, waits for them, and re-layouts  28.6 us (9%)
  matrix products  28.4 us (9%)
  other arithmetic  24.4 us (8%)
  between operations  15.8 us (5%)
    psum x3, waiting for transfers between devices, broadcast_by_axis(): value = lax.psum(value, axis)  110 us
    all_gather x3, waiting for transfers between devices, entering(): pieces = jax.tree.map(lambda part: lax.all_gather(part, axis), so_far)  58.1 us
    all_gather x3, blocking collectives, entering(): pieces = jax.tree.map(lambda part: lax.all_gather(part, axis), so_far)  36.5 us
    reshape x5, local copies, waits for them, and re-layouts, to_blocks(): values.reshape(blocks, BLOCK, head_count, values.shape[1] // head_count)  20.6 us
    all_to_all x1, blocking collectives, per_device(): lax.all_to_all(gated, 'tp', split_axis=0, concat_axis=1, tiled=True)  10.4 us
    dot_general x1, matrix products, per_device(): within = jnp.einsum('nhcs,nshv->nchv', scores, written_update)  8.21 us
    dot_general x1, matrix products, per_device(): jnp.dot(regrouped, lax.all_gather(out_weight, 'tp', axis=0, tiled=True),...  7.04 us
  transfers between devices with their start and end apart: 7, of which 5 were waited for; matrix products, arithmetic and copies ran while one was open for 15% of the time, Pallas kernels for 0%

commit v1 on v0

v1 whole, which is shorter than its diff:
```python
import functools

import jax
import jax.numpy as jnp
from jax import lax
from jax.experimental import pallas as pl
from jax.experimental.pallas import tpu as pltpu
from jax.sharding import Mesh
from jax.sharding import PartitionSpec as P

BLOCK = 128
EPSILON = 1e-06
Z, Y, X = ("sp_0", "sp_1", "sp_2")
SP = (Z, Y, X)
PLANE = (Y, X)
SP_TP = (Z, Y, X, "tp")
F32 = jnp.float32
BF16 = jnp.bfloat16


def mm(a, b, dims=((1,), (0,))):
    return lax.dot_general(a, b, (dims, ((), ())), preferred_element_type=F32)


def iota(shape, axis):
    return lax.broadcasted_iota(jnp.int32, shape, axis)


def params(limit_mib):
    return pltpu.CompilerParams(
        dimension_semantics=("arbitrary",), vmem_limit_bytes=limit_mib * 1024 * 1024
    )


def deal_matrix(plane, depth, transposed):
    rows = plane * depth
    dealt = iota((rows, rows), 1 if transposed else 0)
    natural = iota((rows, rows), 0 if transposed else 1)
    return ((dealt % depth) * plane + dealt // depth == natural).astype(BF16)


def state_kernel(heads, plane, depth, gap, logit, value, key_out, grow_out, start_out, offset_out,
                 send_out, state, decay, pair):
    step = pl.program_id(0)

    @pl.when(step == 0)
    def _():
        state[...] = jnp.zeros_like(state)
        decay[...] = jnp.ones_like(decay)

    lower = (iota((BLOCK, BLOCK), 0) >= iota((BLOCK, BLOCK), 1)).astype(BF16)
    lower2 = jnp.concatenate([lower, lower], axis=1)
    for b in range(logit.shape[0] // BLOCK):
        rows = pl.ds(b * BLOCK, BLOCK)
        key_gate = gap[...] * jax.nn.sigmoid(-logit[rows, :].astype(F32))
        log_forget = jnp.log1p(-key_gate)
        high = log_forget.astype(BF16)
        low = (log_forget - high.astype(F32)).astype(BF16)
        cumul = mm(lower2, jnp.concatenate([high, low], axis=0))
        grow = jnp.exp(cumul)
        key = (key_gate * jnp.exp(-cumul)).astype(BF16)
        grow_out[rows, :] = grow
        key_out[rows, :] = key
        start_out[b] = state[...].astype(BF16)
        offset_out[b] = decay[...]
        block_decay = grow[BLOCK - 1 :, :]
        for h in range(heads):
            cols = pl.ds(h * 128, 128)
            update = mm(value[rows, cols], key[:, h * 128 : (h + 1) * 128], ((0,), (0,)))
            state[:, cols] = block_decay[:, h * 128 : (h + 1) * 128] * (state[:, cols] + update)
        decay[...] = decay[...] * block_decay

    @pl.when(step == pl.num_programs(0) - 1)
    def _():
        deal = deal_matrix(plane, depth, False)
        for h in range(heads):
            cols = pl.ds(h * 128, 128)
            dealt = mm(deal, state[:, cols].astype(BF16), ((1,), (1,)))
            send_out[:, h * depth : (h + 1) * depth, :] = (
                dealt.reshape(plane, depth, 128).astype(BF16)
            )
            whole = decay[:, cols]
            high = whole.astype(BF16).astype(F32)
            pair[h : h + 1, :] = high
            pair[heads + h : heads + h + 1, :] = whole - high
        tail = pair[...].astype(BF16)
        for p in range(plane):
            send_out[p, heads * depth :, :] = tail


def local_state(gap, logit, value, heads, plane, depth, rows):
    span, width = logit.shape
    blocks = rows // BLOCK
    tall = pl.BlockSpec((rows, width), lambda i: (i, 0))
    whole = pl.BlockSpec((1, width), lambda i: (0, 0))
    sent = (plane, heads * depth + 2 * heads, 128)
    return pl.pallas_call(
        functools.partial(state_kernel, heads, plane, depth),
        grid=(span // rows,),
        in_specs=[whole, tall, tall],
        out_specs=[
            tall,
            tall,
            pl.BlockSpec((blocks, 128, width), lambda i: (i, 0, 0)),
            pl.BlockSpec((blocks, 1, width), lambda i: (i, 0, 0)),
            pl.BlockSpec(sent, lambda i: (0, 0, 0)),
        ],
        out_shape=[
            jax.ShapeDtypeStruct((span, width), BF16),
            jax.ShapeDtypeStruct((span, width), F32),
            jax.ShapeDtypeStruct((span // BLOCK, 128, width), BF16),
            jax.ShapeDtypeStruct((span // BLOCK, 1, width), F32),
            jax.ShapeDtypeStruct(sent, BF16),
        ],
        scratch_shapes=[
            pltpu.VMEM((128, width), F32),
            pltpu.VMEM((1, width), F32),
            pltpu.VMEM((2 * heads, 128), F32),
        ],
        compiler_params=params(24),
        cost_estimate=pl.CostEstimate(flops=6_000_000_000, bytes_accessed=10_000_000, transcendentals=0),
        name="stretch_state",
    )(gap, logit, value)


def output_kernel(heads, which, query, key, grow, value, start, offset, gate, gain,
                  raw_out, reach_out, gated_out):
    causal = iota((BLOCK, BLOCK), 0) >= iota((BLOCK, BLOCK), 1)
    for b in range(query.shape[0] // BLOCK):
        rows = pl.ds(b * BLOCK, BLOCK)
        for h in range(heads):
            cols = pl.ds(h * 128, 128)
            reader = jax.nn.silu(query[rows, cols].astype(F32)) * grow[rows, cols]
            reader_low = reader.astype(BF16)
            reach_out[rows, cols] = (reader * offset[b][:, h * 128 : (h + 1) * 128]).astype(BF16)
            scores = mm(reader_low, key[rows, cols], ((1,), (1,)))
            scores = jnp.where(causal, scores, 0.0).astype(BF16)
            raw_out[rows, cols] = mm(scores, value[rows, cols]) + mm(
                reader_low, start[b, :, cols], ((1,), (1,))
            )
            gated_out[rows, cols] = jax.nn.silu(gate[rows, cols].astype(F32)) * gain[:, cols]


def local_output(which, query, key, grow, value, start, offset, gate, gain, heads, rows):
    span, width = query.shape
    half = span // 2
    steps = half // rows
    blocks = rows // BLOCK
    read = pl.BlockSpec((rows, width), lambda i, w: (w[0] * steps + i, 0))
    write = pl.BlockSpec((rows, width), lambda i, w: (i, 0))
    return pl.pallas_call(
        functools.partial(output_kernel, heads),
        grid_spec=pltpu.PrefetchScalarGridSpec(
            num_scalar_prefetch=1,
            grid=(steps,),
            in_specs=[
                read,
                read,
                read,
                read,
                pl.BlockSpec((blocks, 128, width), lambda i, w: (w[0] * steps + i, 0, 0)),
                pl.BlockSpec((blocks, 1, width), lambda i, w: (w[0] * steps + i, 0, 0)),
                read,
                pl.BlockSpec((1, width), lambda i, w: (0, 0)),
            ],
            out_specs=[write, write, write],
        ),
        out_shape=[
            jax.ShapeDtypeStruct((half, width), F32),
            jax.ShapeDtypeStruct((half, width), BF16),
            jax.ShapeDtypeStruct((half, width), F32),
        ],
        compiler_params=params(24),
        cost_estimate=pl.CostEstimate(flops=6_000_000_000, bytes_accessed=10_000_000, transcendentals=0),
        name="stretch_output",
    )(which, query, key, grow, value, start, offset, gate, gain)


def decay_columns(place, received, heads, depth, plane):
    count = received.shape[0]
    picked = (iota((depth, 128), 1) == iota((depth, 128), 0) * plane + place).astype(BF16)
    parts = received[:, heads * depth :, :].reshape(count * 2 * heads, 128)
    columns = mm(picked, parts, ((1,), (1,)))
    lanes = columns.shape[1]
    return columns + pltpu.roll(columns, lanes - heads, 1)


def plane_kernel(heads, plane, depth, place, received, send_out, prefix_out, product_out):
    columns = decay_columns(place[0], received, heads, depth, plane)
    total = None
    states = [jnp.zeros((depth, 128), F32) for _ in range(heads)]
    products = [jnp.ones((depth, 128), F32) for _ in range(heads)]
    for s in range(plane):
        parts = received[s, heads * depth :, :].astype(F32)
        row_decay = parts + pltpu.roll(parts, heads, 0)
        total = row_decay if total is None else total * row_decay
        for h in range(heads):
            rows = slice(h * depth, (h + 1) * depth)
            prefix_out[s, rows, :] = states[h]
            product_out[s, rows, :] = products[h]
            lane = s * 2 * heads + h
            decay = jnp.broadcast_to(columns[:, lane : lane + 1], (depth, 128))
            states[h] = decay * states[h] + received[s, rows, :].astype(F32)
            products[h] = decay * products[h]
    high = total.astype(BF16).astype(F32)
    tail = jnp.where(iota(total.shape, 0) < heads, high, total - high).astype(BF16)
    for d in range(send_out.shape[0]):
        for h in range(heads):
            send_out[d, h * depth : (h + 1) * depth, :] = states[h].astype(BF16)
        send_out[d, heads * depth :, :] = tail


def plane_scan(place, received, heads, depth):
    plane, tall, _ = received.shape
    rows = heads * depth
    return pl.pallas_call(
        functools.partial(plane_kernel, heads, plane, depth),
        grid_spec=pltpu.PrefetchScalarGridSpec(
            num_scalar_prefetch=1,
            grid=(1,),
            in_specs=[pl.BlockSpec((plane, tall, 128), lambda i, w: (0, 0, 0))],
            out_specs=[
                pl.BlockSpec((depth, tall, 128), lambda i, w: (0, 0, 0)),
                pl.BlockSpec((plane, rows, 128), lambda i, w: (0, 0, 0)),
                pl.BlockSpec((plane, rows, 128), lambda i, w: (0, 0, 0)),
            ],
        ),
        out_shape=[
            jax.ShapeDtypeStruct((depth, tall, 128), BF16),
            jax.ShapeDtypeStruct((plane, rows, 128), F32),
            jax.ShapeDtypeStruct((plane, rows, 128), F32),
        ],
        compiler_params=params(8),
        cost_estimate=pl.CostEstimate(flops=100_000_000, bytes_accessed=1_000_000, transcendentals=0),
        name="plane_scan",
    )(place, received)


def depth_kernel(heads, plane, depth, place, received, prefix, product, first, send_out, final_out,
                 entering, final):
    columns = decay_columns(place[0], received, heads, depth, plane)
    states = [first[h] for h in range(heads)]
    for s in range(depth):
        for h in range(heads):
            rows = slice(h * depth, (h + 1) * depth)
            entering[s, rows, :] = states[h]
            lane = s * 2 * heads + h
            decay = jnp.broadcast_to(columns[:, lane : lane + 1], (depth, 128))
            states[h] = decay * states[h] + received[s, rows, :].astype(F32)
    for h in range(heads):
        final[h] = states[h]
        final_out[h : h + 1, :] = final[h, pl.ds(place[1], 1), :]
    mine = entering[place[1]]
    for p in range(plane):
        send_out[p] = (prefix[p] + product[p] * mine).astype(BF16)


def depth_scan(place, received, prefix, product, first, heads):
    depth, tall, _ = received.shape
    plane, rows, _ = prefix.shape
    return pl.pallas_call(
        functools.partial(depth_kernel, heads, plane, depth),
        grid_spec=pltpu.PrefetchScalarGridSpec(
            num_scalar_prefetch=1,
            grid=(1,),
            in_specs=[
                pl.BlockSpec((depth, tall, 128), lambda i, w: (0, 0, 0)),
                pl.BlockSpec((plane, rows, 128), lambda i, w: (0, 0, 0)),
                pl.BlockSpec((plane, rows, 128), lambda i, w: (0, 0, 0)),
                pl.BlockSpec((heads, depth, 128), lambda i, w: (0, 0, 0)),
            ],
            out_specs=[
                pl.BlockSpec((plane, rows, 128), lambda i, w: (0, 0, 0)),
                pl.BlockSpec((heads, 128), lambda i, w: (0, 0)),
            ],
            scratch_shapes=[
                pltpu.VMEM((depth, rows, 128), F32),
                pltpu.VMEM((heads, depth, 128), F32),
            ],
        ),
        out_shape=[
            jax.ShapeDtypeStruct((plane, rows, 128), BF16),
            jax.ShapeDtypeStruct((heads, 128), F32),
        ],
        compiler_params=params(8),
        cost_estimate=pl.CostEstimate(flops=100_000_000, bytes_accessed=1_000_000, transcendentals=0),
        name="depth_scan",
    )(place, received, prefix, product, first)


def finish_kernel(heads, depth, incoming, raw, reach, gating, gated_out, state):
    plane = incoming.shape[0]

    @pl.when(pl.program_id(0) == 0)
    def _():
        collect = deal_matrix(plane, depth, True)
        for h in range(heads):
            part = incoming[:, h * depth : (h + 1) * depth, :].astype(F32)
            part = part.reshape(plane * depth, 128).astype(BF16)
            state[h] = mm(collect, part).astype(BF16)

    mean = jnp.full((128, 128), 1.0 / 128, BF16)
    for b in range(raw.shape[0] // BLOCK):
        rows = pl.ds(b * BLOCK, BLOCK)
        for h in range(heads):
            cols = pl.ds(h * 128, 128)
            value = raw[rows, cols] + mm(reach[rows, cols], state[h])
            mean_square = mm((value * value).astype(BF16), mean)
            gated_out[rows, cols] = (
                value * lax.rsqrt(mean_square + EPSILON) * gating[rows, cols]
            ).astype(BF16)


def finish(incoming, raw, reach, gating, heads, depth, rows):
    span, width = raw.shape
    tall = pl.BlockSpec((rows, width), lambda i: (i, 0))
    return pl.pallas_call(
        functools.partial(finish_kernel, heads, depth),
        grid=(span // rows,),
        in_specs=[pl.BlockSpec(incoming.shape, lambda i: (0, 0, 0)), tall, tall, tall],
        out_specs=tall,
        out_shape=jax.ShapeDtypeStruct((span, width), BF16),
        scratch_shapes=[pltpu.VMEM((heads, 128, 128), BF16)],
        compiler_params=params(16),
        cost_estimate=pl.CostEstimate(flops=2_000_000_000, bytes_accessed=4_000_000, transcendentals=0),
        name="finish",
    )(incoming, raw, reach, gating)


def project_kernel(mine, theirs, my_weight, their_weight, out):
    total = mm(mine[...], my_weight[...]) + mm(theirs[...], their_weight[...])
    out[...] = total.astype(BF16)


def project(mine, theirs, my_weight, their_weight, cols):
    rows, inner = mine.shape
    width = my_weight.shape[1]
    left = pl.BlockSpec((rows, inner), lambda i: (0, 0))
    right = pl.BlockSpec((inner, cols), lambda i: (0, i))
    return pl.pallas_call(
        project_kernel,
        grid=(width // cols,),
        in_specs=[left, left, right, right],
        out_specs=pl.BlockSpec((rows, cols), lambda i: (0, i)),
        out_shape=jax.ShapeDtypeStruct((rows, width), BF16),
        compiler_params=params(24),
        cost_estimate=pl.CostEstimate(flops=3_300_000_000, bytes_accessed=9_000_000, transcendentals=0),
        name="project",
    )(mine, theirs, my_weight, their_weight)


def per_device(
    queries, forget_logit, value_rows, out_gate, floor_gap, head_gain, state_in, out_weight
):
    heads = state_in.shape[0]
    plane = lax.axis_size(PLANE)
    depth = lax.axis_size(Z)
    place_plane = lax.axis_index(PLANE)
    place = jnp.stack([place_plane, lax.axis_index(Z)]).astype(jnp.int32)
    core = lax.axis_index("tp")
    other_half = (1 - core).reshape(1).astype(jnp.int32)
    my_half = core.reshape(1).astype(jnp.int32)
    swap = [(0, 1), (1, 0)]
    barrier = lax.optimization_barrier

    their_weight = lax.ppermute(out_weight, "tp", swap)
    gap = floor_gap.reshape(1, -1)
    gain = head_gain.reshape(1, -1)
    first = lax.dynamic_index_in_dim(
        state_in.reshape(heads, depth, plane, 128), place_plane, 2, keepdims=False
    )

    key, grow, start, offset, send = local_state(
        gap, forget_logit, value_rows, heads, plane, depth, 384
    )
    received = lax.all_to_all(send, PLANE, 0, 0, tiled=True)
    far = local_output(
        other_half, queries, key, grow, value_rows, start, offset, out_gate, gain, heads, 384
    )
    received, far, key = barrier((received, far, key))

    send, prefix, product = plane_scan(place, received, heads, depth)
    received = lax.all_to_all(send, Z, 0, 0, tiled=True)
    near = local_output(
        my_half, queries, key, grow, value_rows, start, offset, out_gate, gain, heads, 384
    )
    received, near = barrier((received, near))

    send, state_out = depth_scan(place, received, prefix, product, first, heads)
    incoming = lax.all_to_all(send, PLANE, 0, 0, tiled=True)

    far_gated = finish(incoming, *far, heads, depth, 384)
    theirs = lax.ppermute(far_gated, "tp", swap)
    mine = finish(incoming, *near, heads, depth, 384)
    projected = project(mine, theirs, out_weight, their_weight, 256)
    return (projected, state_out)


def solution(mesh):
    torus = Mesh(mesh.devices.reshape(8, 4, 4, mesh.shape["tp"]), (Z, Y, X, "tp"))
    placed = (
        P(SP, "tp"),
        P(SP, "tp"),
        P(SP, "tp"),
        P(SP, "tp"),
        P("tp"),
        P("tp"),
        P("tp", None, None),
        P("tp", None),
    )
    return jax.shard_map(
        per_device,
        mesh=torus,
        in_specs=placed,
        out_specs=(P(SP_TP, None), P("tp", SP)),
        check_vma=False,
    )
```

time: 315 us -> 95.3 us (0.30)
  waiting for transfers between devices: 168 us -> 0.76 us
  blocking collectives: 47 us -> 13.6 us
  matrix products: 28.4 us -> 0 us
  Pallas kernels: 0 us -> 24.7 us
  other arithmetic: 24.4 us -> 0.07 us
  starting transfers between devices: 0.47 us -> 18.6 us
  between operations: 15.8 us -> 0.76 us
  local copies, waits for them, and re-layouts: 28.6 us -> 35.9 us
    psum x3 -> x0, waiting for transfers between devices: 110 us -> none  [broadcast_by_axis(): value = lax.psum(value, axis)]
    all_gather x4 -> x0, waiting for transfers between devices: 58.2 us -> none  [the longest x3 58.1 us: entering(): pieces = jax.tree.map(lambda part: lax.all_gather(part, axis), so_far)]
    all_gather x3 -> x0, blocking collectives: 36.5 us -> none  [entering(): pieces = jax.tree.map(lambda part: lax.all_gather(part, axis), so_far)]
    unnamed x11 -> x66, local copies, waits for them, and re-layouts: 3.59 us -> 35.9 us
    dot_general x7 -> x0, matrix products: 28.4 us -> none  [the longest x1 8.21 us: per_device(): within = jnp.einsum('nhcs,nshv->nchv', scores, written_update)]
    pallas_call x0 -> x8, Pallas kernels: none -> 24.7 us  [the longest x1 8.02 us: project(): pl.pallas_call(project_kernel, grid=(width // cols,), in_specs=[left, lef...]
    reshape x5 -> x0, local copies, waits for them, and re-layouts: 20.6 us -> none  [to_blocks(): values.reshape(blocks, BLOCK, head_count, values.shape[1] // head_count)]
    all_to_all x0 -> x2, starting transfers between devices: none -> 15.8 us  [the longest x1 8.18 us: per_device(): received = lax.all_to_all(send, Z, 0, 0, tiled=True)]
  transfers between devices with their start and end apart: 7 -> 4, of which waited for: 5 -> 1; matrix products, arithmetic and copies ran while one was open for 15% -> 0% of each run, Pallas kernels for 0% -> 11%
where the time goes in v1:
time: 95.3 us; the launch traced here: 94.3 us
  local copies, waits for them, and re-layouts  35.9 us (38%)
  Pallas kernels  24.7 us (26%)
  starting transfers between devices  18.6 us (20%)
  blocking collectives  13.6 us (14%)
    unnamed x66, local copies, waits for them, and re-layouts  35.9 us
    all_to_all x1, blocking collectives, per_device(): incoming = lax.all_to_all(send, PLANE, 0, 0, tiled=True)  13.6 us
    all_to_all x1, starting transfers between devices, per_device(): received = lax.all_to_all(send, Z, 0, 0, tiled=True)  8.18 us
    pallas_call x1, Pallas kernels, project(): pl.pallas_call(project_kernel, grid=(width // cols,), in_specs=[left, lef...  8.02 us
    all_to_all x1, starting transfers between devices, per_device(): received = lax.all_to_all(send, PLANE, 0, 0, tiled=True)  7.58 us
    pallas_call x1, Pallas kernels, local_state(): pl.pallas_call(functools.partial(state_kernel, heads, plane, depth), grid...  6.05 us
    pallas_call x2, Pallas kernels, local_output(): pl.pallas_call(functools.partial(output_kernel, heads), grid_spec=pltpu.P...  5.16 us
    pallas_call x2, Pallas kernels, finish(): pl.pallas_call(functools.partial(finish_kernel, heads, depth), grid=(span...  2.28 us
  transfers between devices with their start and end apart: 4, of which 1 were waited for; matrix products, arithmetic and copies ran while one was open for 0% of the time, Pallas kernels for 11%

profile of v1, /device:TPU:1, one launch (start us, length us, event | category | flops | bytes accessed | tf_op | source)
XLA Modules:
  0.0 94.3 jit_solution(8115681169410641648)
XLA Ops:
  0.6 0.0 copy-start
  0.7 1.4 %copy-done.2 = bf16[1536,512]{1,0:T(8,128)(2,1)S(1)} copy-done((bf16[1536,512]{1,0:T(8,128)(2,1)S(1)}, bf16[1536,512]{1,0:T(8,128)(2,1)}, u32[]{:S(2)}) %copy-start.2) | copy-done | bytes 1572888
  2.1 1.4 %copy-done.3 = bf16[1536,512]{1,0:T(8,128)(2,1)S(1)} copy-done((bf16[1536,512]{1,0:T(8,128)(2,1)S(1)}, bf16[1536,512]{1,0:T(8,128)(2,1)}, u32[]{:S(2)}) %copy-start.3) | copy-done | bytes 1572888
  3.5 0.7 copy-done.10
  4.2 6.0 %stretch_state.1 = (bf16[1536,512]{1,0:T(8,128)(2,1)S(1)}, f32[1536,512]{1,0:T(8,128)S(1)}, bf16[12,128,512]{2,1,0:T(8,128)(2,1)S(1)}, f32[12,1,512]{2,1,0:T(1,128)S(1)}, bf16[16,40,128]{2,1,0:T(8,128)(2,1)}) custom-call(f32[1,512]{1,0:T(1,128)S(1)} %bitcast.12, bf16[1536,512]{1,0:T(8,128)(2,1)S(1)} %copy-done.2, bf16[1536,512]{1,0:T(8,128)(2,1)S(1)} %copy-done.3), custom_call_target="tpu_custom_call" | custom-call | flops 6000000000 | bytes 10000000 | tf_op jit(solution)/shard_map/stretch_state/pallas_call | solution.py:97
  10.2 1.7 %copy-done.24 = f32[1536,512]{1,0:T(8,128)} copy-done((f32[1536,512]{1,0:T(8,128)}, f32[1536,512]{1,0:T(8,128)S(1)}, u32[]{:S(2)}) %copy-start.24) | copy-done | bytes 3145752
  11.9 1.2 %copy-done.27 = bf16[1536,512]{1,0:T(8,128)(2,1)} copy-done((bf16[1536,512]{1,0:T(8,128)(2,1)}, bf16[1536,512]{1,0:T(8,128)(2,1)S(1)}, u32[]{:S(2)}) %copy-start.27) | copy-done | bytes 1572888
  13.1 1.2 %copy-done.30 = bf16[12,128,512]{2,1,0:T(8,128)(2,1)} copy-done((bf16[12,128,512]{2,1,0:T(8,128)(2,1)}, bf16[12,128,512]{2,1,0:T(8,128)(2,1)S(1)}, u32[]{:S(2)}) %copy-start.30) | copy-done | bytes 1572888
  14.3 7.6 %all-to-all-start = ((bf16[16,40,128]{2,1,0:T(8,128)(2,1)}), bf16[16,40,128]{2,1,0:T(8,128)(2,1)S(1)}, u32[]{:S(2)}, u32[]{:S(2)}) async-start(bf16[16,40,128]{2,1,0:T(8,128)(2,1)} %get-tuple-element.27), calls=%async_computation | async-start | bytes 327680 | tf_op jit(solution)/shard_map/all_to_all | solution.py:376
  21.9 1.0 %collective-permute-start.1 = (bf16[512,2048]{1,0:T(8,128)(2,1)S(1)}, bf16[512,2048]{1,0:T(8,128)(2,1)}, u32[]{:S(2)}, u32[]{:S(2)}) collective-permute-start(bf16[512,2048]{1,0:T(8,128)(2,1)S(1)} %copy-done.1), channel_id=1, source_target_pairs={{0,1},{1,0},{2,3},{3,2},{4,5},{5,4},{6,7},{7,6},{8,9},{9,8},{10,11... | collective-permute-start | bytes 6291464 | tf_op jit(solution)/shard_map/ppermute | solution.py:366
  23.0 1.4 %copy-done.4 = bf16[1536,512]{1,0:T(8,128)(2,1)S(1)} copy-done((bf16[1536,512]{1,0:T(8,128)(2,1)S(1)}, bf16[1536,512]{1,0:T(8,128)(2,1)}, u32[]{:S(2)}) %copy-start.4) | copy-done | bytes 1572888
  24.4 1.4 %copy-done.6 = bf16[1536,512]{1,0:T(8,128)(2,1)S(1)} copy-done((bf16[1536,512]{1,0:T(8,128)(2,1)S(1)}, bf16[1536,512]{1,0:T(8,128)(2,1)}, u32[]{:S(2)}) %copy-start.6) | copy-done | bytes 1572888
  25.8 1.4 %copy-done.8 = bf16[1536,512]{1,0:T(8,128)(2,1)S(1)} copy-done((bf16[1536,512]{1,0:T(8,128)(2,1)S(1)}, bf16[1536,512]{1,0:T(8,128)(2,1)}, u32[]{:S(2)}) %copy-start.8) | copy-done | bytes 1572888
  27.2 1.9 %copy-done.25 = f32[1536,512]{1,0:T(8,128)S(1)} copy-done((f32[1536,512]{1,0:T(8,128)S(1)}, f32[1536,512]{1,0:T(8,128)}, u32[]{:S(2)}) %copy-start.25) | copy-done | bytes 3145752
  29.1 1.4 %copy-done.28 = bf16[1536,512]{1,0:T(8,128)(2,1)S(1)} copy-done((bf16[1536,512]{1,0:T(8,128)(2,1)S(1)}, bf16[1536,512]{1,0:T(8,128)(2,1)}, u32[]{:S(2)}) %copy-start.28) | copy-done | bytes 1572888
  30.5 1.4 %copy-done.31 = bf16[12,128,512]{2,1,0:T(8,128)(2,1)S(1)} copy-done((bf16[12,128,512]{2,1,0:T(8,128)(2,1)S(1)}, bf16[12,128,512]{2,1,0:T(8,128)(2,1)}, u32[]{:S(2)}) %copy-start.31) | copy-done | bytes 1572888
  31.9 2.6 %stretch_output.2 = (f32[768,512]{1,0:T(8,128)S(1)}, bf16[768,512]{1,0:T(8,128)(2,1)S(1)}, f32[768,512]{1,0:T(8,128)S(1)}) custom-call(s32[1]{0:T(128)} %bitcast.3.which, bf16[1536,512]{1,0:T(8,128)(2,1)S(1)} %copy-done.6, bf16[1536,512]{1,0:T(8,128)(2,1)S(1)} %copy-done.28, f32[1536,512]{1,0:T(8,128)S(1)} %copy-done.25, bf16[1536,512]{1,0:T(8,128)(2,1)S(1)} %copy-done.4, ...), custom_call_target="tpu_custom_call" | custom-call | flops 6000000000 | bytes 10000000 | tf_op jit(solution)/shard_map/stretch_output/pallas_call | solution.py:151
  34.5 1.2 %copy-done.12 = f32[768,512]{1,0:T(8,128)} copy-done((f32[768,512]{1,0:T(8,128)}, f32[768,512]{1,0:T(8,128)S(1)}, u32[]{:S(2)}) %copy-start.12) | copy-done | bytes 1572888
  35.6 1.2 %copy-done.14 = f32[768,512]{1,0:T(8,128)} copy-done((f32[768,512]{1,0:T(8,128)}, f32[768,512]{1,0:T(8,128)S(1)}, u32[]{:S(2)}) %copy-start.14) | copy-done | bytes 1572888
  36.8 0.9 copy-done.20
  37.7 0.1 pad_add_fusion.place
  37.8 0.0 all-to-all-done.received
  37.8 1.6 %plane_scan.1 = (bf16[8,40,128]{2,1,0:T(8,128)(2,1)}, f32[16,32,128]{2,1,0:T(8,128)S(1)}, f32[16,32,128]{2,1,0:T(8,128)S(1)}) custom-call(s32[2]{0:T(128)S(1)} %pad_add_fusion.place, bf16[16,40,128]{2,1,0:T(8,128)(2,1)S(1)} %all-to-all-done.received), custom_call_target="tpu_custom_call" | custom-call | flops 100000000 | bytes 1000000 | tf_op jit(solution)/shard_map/plane_scan/pallas_call | solution.py:216
  39.4 8.2 %all-to-all-start.1 = ((bf16[8,40,128]{2,1,0:T(8,128)(2,1)}), bf16[8,40,128]{2,1,0:T(8,128)(2,1)S(1)}, u32[]{:S(2)}, u32[]{:S(2)}) async-start(bf16[8,40,128]{2,1,0:T(8,128)(2,1)} %get-tuple-element.36), calls=%async_computation.1 | async-start | bytes 163840 | tf_op jit(solution)/shard_map/all_to_all | solution.py:383
  47.6 1.4 %copy-done.5 = bf16[1536,512]{1,0:T(8,128)(2,1)S(1)} copy-done((bf16[1536,512]{1,0:T(8,128)(2,1)S(1)}, bf16[1536,512]{1,0:T(8,128)(2,1)}, u32[]{:S(2)}) %copy-start.5) | copy-done | bytes 1572888
  49.0 1.4 %copy-done.7 = bf16[1536,512]{1,0:T(8,128)(2,1)S(1)} copy-done((bf16[1536,512]{1,0:T(8,128)(2,1)S(1)}, bf16[1536,512]{1,0:T(8,128)(2,1)}, u32[]{:S(2)}) %copy-start.7) | copy-done | bytes 1572888
  50.4 1.4 %copy-done.9 = bf16[1536,512]{1,0:T(8,128)(2,1)S(1)} copy-done((bf16[1536,512]{1,0:T(8,128)(2,1)S(1)}, bf16[1536,512]{1,0:T(8,128)(2,1)}, u32[]{:S(2)}) %copy-start.9) | copy-done | bytes 1572888
  51.8 1.9 %copy-done.26 = f32[1536,512]{1,0:T(8,128)S(1)} copy-done((f32[1536,512]{1,0:T(8,128)S(1)}, f32[1536,512]{1,0:T(8,128)}, u32[]{:S(2)}) %copy-start.26) | copy-done | bytes 3145752
  53.7 1.4 %copy-done.29 = bf16[1536,512]{1,0:T(8,128)(2,1)S(1)} copy-done((bf16[1536,512]{1,0:T(8,128)(2,1)S(1)}, bf16[1536,512]{1,0:T(8,128)(2,1)}, u32[]{:S(2)}) %copy-start.29) | copy-done | bytes 1572888
  55.1 1.4 %copy-done.32 = bf16[12,128,512]{2,1,0:T(8,128)(2,1)S(1)} copy-done((bf16[12,128,512]{2,1,0:T(8,128)(2,1)S(1)}, bf16[12,128,512]{2,1,0:T(8,128)(2,1)}, u32[]{:S(2)}) %copy-start.32) | copy-done | bytes 1572888
  56.5 2.6 %stretch_output.3 = (f32[768,512]{1,0:T(8,128)S(1)}, bf16[768,512]{1,0:T(8,128)(2,1)S(1)}, f32[768,512]{1,0:T(8,128)S(1)}) custom-call(s32[1]{0:T(128)} %bitcast.5.which, bf16[1536,512]{1,0:T(8,128)(2,1)S(1)} %copy-done.7, bf16[1536,512]{1,0:T(8,128)(2,1)S(1)} %copy-done.29, f32[1536,512]{1,0:T(8,128)S(1)} %copy-done.26, bf16[1536,512]{1,0:T(8,128)(2,1)S(1)} %copy-done.5, ...), custom_call_target="tpu_custom_call" | custom-call | flops 6000000000 | bytes 10000000 | tf_op jit(solution)/shard_map/stretch_output/pallas_call | solution.py:151
  59.1 0.0 copy-start.16
  59.1 1.1 %copy-done.16 = f32[768,512]{1,0:T(8,128)} copy-done((f32[768,512]{1,0:T(8,128)}, f32[768,512]{1,0:T(8,128)S(1)}, u32[]{:S(2)}) %copy-start.16) | copy-done | bytes 1572888
  60.3 1.2 %copy-done.18 = f32[768,512]{1,0:T(8,128)} copy-done((f32[768,512]{1,0:T(8,128)}, f32[768,512]{1,0:T(8,128)S(1)}, u32[]{:S(2)}) %copy-start.18) | copy-done | bytes 1572888
  61.4 0.9 copy-done.22
  62.3 0.0 all-to-all-done.1.received
  62.3 1.6 %depth_scan.1 = (bf16[16,32,128]{2,1,0:T(8,128)(2,1)S(1)}, f32[4,128]{1,0:T(4,128)}) custom-call(s32[2]{0:T(128)S(1)} %pad_add_fusion.place, bf16[8,40,128]{2,1,0:T(8,128)(2,1)S(1)} %all-to-all-done.1.received, f32[16,32,128]{2,1,0:T(8,128)S(1)} %get-tuple-element.42.prefix, f32[16,32,128]{2,1,0:T(8,128)S(1)} %get-tuple-element.43.product, ...), custom_call_target="tpu_custom_call" | custom-call | flops 100000000 | bytes 1000000 | tf_op jit(solution)/shard_map/depth_scan/pallas_call | solution.py:261
  63.9 13.6 %all_to_all.15.incoming = bf16[16,32,128]{2,1,0:T(8,128)(2,1)S(1)} all-to-all(bf16[16,32,128]{2,1,0:T(8,128)(2,1)S(1)} %get-tuple-element.44), channel_id=1, replica_groups=mesh['sp_0'=8,'sp_1'=4,'sp_2'=4,'tp'=2] {'sp_1','sp_2'}, dimensions={0} | all-to-all | bytes 262144 | tf_op jit(solution)/shard_map/all_to_all | solution.py:390
  77.5 1.4 %copy-done.13 = f32[768,512]{1,0:T(8,128)S(1)} copy-done((f32[768,512]{1,0:T(8,128)S(1)}, f32[768,512]{1,0:T(8,128)}, u32[]{:S(2)}) %copy-start.13) | copy-done | bytes 1572888
  78.9 1.4 %copy-done.15 = f32[768,512]{1,0:T(8,128)S(1)} copy-done((f32[768,512]{1,0:T(8,128)S(1)}, f32[768,512]{1,0:T(8,128)}, u32[]{:S(2)}) %copy-start.15) | copy-done | bytes 1572888
  80.3 1.1 %copy-done.21 = bf16[768,512]{1,0:T(8,128)(2,1)S(1)} copy-done((bf16[768,512]{1,0:T(8,128)(2,1)S(1)}, bf16[768,512]{1,0:T(8,128)(2,1)}, u32[]{:S(2)}) %copy-start.21) | copy-done | bytes 786456
  81.4 1.1 %finish.3 = bf16[768,512]{1,0:T(8,128)(2,1)S(1)} custom-call(bf16[16,32,128]{2,1,0:T(8,128)(2,1)S(1)} %all_to_all.15.incoming, f32[768,512]{1,0:T(8,128)S(1)} %copy-done.13, bf16[768,512]{1,0:T(8,128)(2,1)S(1)} %copy-done.21, f32[768,512]{1,0:T(8,128)S(1)} %copy-done.15), custom_call_target="tpu_custom_call" | custom-call | flops 2000000000 | bytes 4000000 | tf_op jit(solution)/shard_map/finish/pallas_call | solution.py:317
  82.6 1.8 %collective-permute-start = (bf16[768,512]{1,0:T(8,128)(2,1)S(1)}, bf16[768,512]{1,0:T(8,128)(2,1)S(1)}, u32[]{:S(2)}, u32[]{:S(2)}) collective-permute-start(bf16[768,512]{1,0:T(8,128)(2,1)S(1)} %finish.3), channel_id=1, source_target_pairs={{0,1},{1,0},{2,3},{3,2},{4,5},{5,4},{6,7},{7,6},{8,9},{9,8},{10,11... | collective-permute-start | bytes 2359304 | tf_op jit(solution)/shard_map/ppermute | solution.py:393
  84.4 0.0 copy-done.17
  84.4 1.1 %finish.2.mine = bf16[768,512]{1,0:T(8,128)(2,1)S(1)} custom-call(bf16[16,32,128]{2,1,0:T(8,128)(2,1)S(1)} %all_to_all.15.incoming, f32[768,512]{1,0:T(8,128)S(1)} %copy-done.17, bf16[768,512]{1,0:T(8,128)(2,1)S(1)} %copy-done.23, f32[768,512]{1,0:T(8,128)S(1)} %copy-done.19), custom_call_target="tpu_custom_call" | custom-call | flops 2000000000 | bytes 4000000 | tf_op jit(solution)/shard_map/finish/pallas_call | solution.py:317
  85.5 0.8 collective-permute-done.theirs
  86.3 0.0 collective-permute-done.1.their_weight
  86.3 8.0 %project.1 = bf16[768,2048]{1,0:T(8,128)(2,1)} custom-call(bf16[768,512]{1,0:T(8,128)(2,1)S(1)} %finish.2.mine, bf16[768,512]{1,0:T(8,128)(2,1)S(1)} %collective-permute-done.theirs, bf16[512,2048]{1,0:T(8,128)(2,1)S(1)} %copy-done.1, bf16[512,2048]{1,0:T(8,128)(2,1)} %collective-permute-done.1.their_weight), custom_call_target="tpu_custom_call" | custom-call | flops 3300000000 | bytes 9000000 | tf_op jit(solution)/shard_map/project/pallas_call | solution.py:340
  (37 shorter events, 0.1 us)
Async XLA Ops:
  0.6 37.2 %copy-start = (f32[4,128,128]{2,1,0:T(8,128)S(1)}, f32[4,128,128]{2,1,0:T(8,128)}, u32[]{:S(2)}) copy-start(f32[4,128,128]{2,1,0:T(8,128)} %param.14) | copy-start | bytes 786436
  0.6 1.5 %copy-start.2 = (bf16[1536,512]{1,0:T(8,128)(2,1)S(1)}, bf16[1536,512]{1,0:T(8,128)(2,1)}, u32[]{:S(2)}) copy-start(bf16[1536,512]{1,0:T(8,128)(2,1)} %logit.1) | copy-start | bytes 4718596
  2.1 1.4 %copy-start.3 = (bf16[1536,512]{1,0:T(8,128)(2,1)S(1)}, bf16[1536,512]{1,0:T(8,128)(2,1)}, u32[]{:S(2)}) copy-start(bf16[1536,512]{1,0:T(8,128)(2,1)} %value.5) | copy-start | bytes 4718596
  3.5 0.7 copy-start.10
  4.2 17.7 %copy-start.1 = (bf16[512,2048]{1,0:T(8,128)(2,1)S(1)}, bf16[512,2048]{1,0:T(8,128)(2,1)}, u32[]{:S(2)}) copy-start(bf16[512,2048]{1,0:T(8,128)(2,1)} %my_weight.1) | copy-start | bytes 6291460
  4.2 18.8 %copy-start.11 = (f32[512]{0:T(512)S(1)}, f32[512]{0:T(512)}, u32[]{:S(2)}) copy-start(f32[512]{0:T(512)} %param.13) | copy-start | bytes 6148
  10.2 1.7 %copy-start.24 = (f32[1536,512]{1,0:T(8,128)}, f32[1536,512]{1,0:T(8,128)S(1)}, u32[]{:S(2)}) copy-start(f32[1536,512]{1,0:T(8,128)S(1)} %get-tuple-element.29.grow) | copy-start | bytes 9437188
  11.9 1.2 %copy-start.27 = (bf16[1536,512]{1,0:T(8,128)(2,1)}, bf16[1536,512]{1,0:T(8,128)(2,1)S(1)}, u32[]{:S(2)}) copy-start(bf16[1536,512]{1,0:T(8,128)(2,1)S(1)} %get-tuple-element.37.key) | copy-start | bytes 4718596
  13.1 1.2 %copy-start.30 = (bf16[12,128,512]{2,1,0:T(8,128)(2,1)}, bf16[12,128,512]{2,1,0:T(8,128)(2,1)S(1)}, u32[]{:S(2)}) copy-start(bf16[12,128,512]{2,1,0:T(8,128)(2,1)S(1)} %get-tuple-element.30.start) | copy-start | bytes 4718596
  14.3 23.5 %all-to-all-start = ((bf16[16,40,128]{2,1,0:T(8,128)(2,1)}), bf16[16,40,128]{2,1,0:T(8,128)(2,1)S(1)}, u32[]{:S(2)}, u32[]{:S(2)}) async-start(bf16[16,40,128]{2,1,0:T(8,128)(2,1)} %get-tuple-element.27), calls=%async_computation | async-start | bytes 327680 | tf_op jit(solution)/shard_map/all_to_all | solution.py:376
  21.9 64.4 %collective-permute-start.1 = (bf16[512,2048]{1,0:T(8,128)(2,1)S(1)}, bf16[512,2048]{1,0:T(8,128)(2,1)}, u32[]{:S(2)}, u32[]{:S(2)}) collective-permute-start(bf16[512,2048]{1,0:T(8,128)(2,1)S(1)} %copy-done.1), channel_id=1, source_target_pairs={{0,1},{1,0},{2,3},{3,2},{4,5},{5,4},{6,7},{7,6},{8,9},{9,8},{10,11... | collective-permute-start | bytes 6291464 | tf_op jit(solution)/shard_map/ppermute | solution.py:366
  23.0 1.4 %copy-start.4 = (bf16[1536,512]{1,0:T(8,128)(2,1)S(1)}, bf16[1536,512]{1,0:T(8,128)(2,1)}, u32[]{:S(2)}) copy-start(bf16[1536,512]{1,0:T(8,128)(2,1)} %value.5) | copy-start | bytes 4718596
  24.4 1.4 %copy-start.6 = (bf16[1536,512]{1,0:T(8,128)(2,1)S(1)}, bf16[1536,512]{1,0:T(8,128)(2,1)}, u32[]{:S(2)}) copy-start(bf16[1536,512]{1,0:T(8,128)(2,1)} %query.3) | copy-start | bytes 4718596
  25.8 1.4 %copy-start.8 = (bf16[1536,512]{1,0:T(8,128)(2,1)S(1)}, bf16[1536,512]{1,0:T(8,128)(2,1)}, u32[]{:S(2)}) copy-start(bf16[1536,512]{1,0:T(8,128)(2,1)} %gate.3) | copy-start | bytes 4718596
  27.2 1.9 %copy-start.25 = (f32[1536,512]{1,0:T(8,128)S(1)}, f32[1536,512]{1,0:T(8,128)}, u32[]{:S(2)}) copy-start(f32[1536,512]{1,0:T(8,128)} %copy-done.24) | copy-start | bytes 9437188
  29.1 1.4 %copy-start.28 = (bf16[1536,512]{1,0:T(8,128)(2,1)S(1)}, bf16[1536,512]{1,0:T(8,128)(2,1)}, u32[]{:S(2)}) copy-start(bf16[1536,512]{1,0:T(8,128)(2,1)} %copy-done.27) | copy-start | bytes 4718596
  30.5 1.4 %copy-start.31 = (bf16[12,128,512]{2,1,0:T(8,128)(2,1)S(1)}, bf16[12,128,512]{2,1,0:T(8,128)(2,1)}, u32[]{:S(2)}) copy-start(bf16[12,128,512]{2,1,0:T(8,128)(2,1)} %copy-done.30) | copy-start | bytes 4718596
  34.5 1.2 %copy-start.12 = (f32[768,512]{1,0:T(8,128)}, f32[768,512]{1,0:T(8,128)S(1)}, u32[]{:S(2)}) copy-start(f32[768,512]{1,0:T(8,128)S(1)} %get-tuple-element.48.raw) | copy-start | bytes 4718596
  35.6 1.2 %copy-start.14 = (f32[768,512]{1,0:T(8,128)}, f32[768,512]{1,0:T(8,128)S(1)}, u32[]{:S(2)}) copy-start(f32[768,512]{1,0:T(8,128)S(1)} %get-tuple-element.50.gating) | copy-start | bytes 4718596
  36.8 0.9 copy-start.20
  39.4 22.9 %all-to-all-start.1 = ((bf16[8,40,128]{2,1,0:T(8,128)(2,1)}), bf16[8,40,128]{2,1,0:T(8,128)(2,1)S(1)}, u32[]{:S(2)}, u32[]{:S(2)}) async-start(bf16[8,40,128]{2,1,0:T(8,128)(2,1)} %get-tuple-element.36), calls=%async_computation.1 | async-start | bytes 163840 | tf_op jit(solution)/shard_map/all_to_all | solution.py:383
  47.6 1.4 %copy-start.5 = (bf16[1536,512]{1,0:T(8,128)(2,1)S(1)}, bf16[1536,512]{1,0:T(8,128)(2,1)}, u32[]{:S(2)}) copy-start(bf16[1536,512]{1,0:T(8,128)(2,1)} %value.5) | copy-start | bytes 4718596
  49.0 1.4 %copy-start.7 = (bf16[1536,512]{1,0:T(8,128)(2,1)S(1)}, bf16[1536,512]{1,0:T(8,128)(2,1)}, u32[]{:S(2)}) copy-start(bf16[1536,512]{1,0:T(8,128)(2,1)} %query.3) | copy-start | bytes 4718596
  50.4 1.4 %copy-start.9 = (bf16[1536,512]{1,0:T(8,128)(2,1)S(1)}, bf16[1536,512]{1,0:T(8,128)(2,1)}, u32[]{:S(2)}) copy-start(bf16[1536,512]{1,0:T(8,128)(2,1)} %gate.3) | copy-start | bytes 4718596
  51.8 1.9 %copy-start.26 = (f32[1536,512]{1,0:T(8,128)S(1)}, f32[1536,512]{1,0:T(8,128)}, u32[]{:S(2)}) copy-start(f32[1536,512]{1,0:T(8,128)} %copy-done.24) | copy-start | bytes 9437188
  53.7 1.4 %copy-start.29 = (bf16[1536,512]{1,0:T(8,128)(2,1)S(1)}, bf16[1536,512]{1,0:T(8,128)(2,1)}, u32[]{:S(2)}) copy-start(bf16[1536,512]{1,0:T(8,128)(2,1)} %copy-done.27) | copy-start | bytes 4718596
  55.1 1.4 %copy-start.32 = (bf16[12,128,512]{2,1,0:T(8,128)(2,1)S(1)}, bf16[12,128,512]{2,1,0:T(8,128)(2,1)}, u32[]{:S(2)}) copy-start(bf16[12,128,512]{2,1,0:T(8,128)(2,1)} %copy-done.30) | copy-start | bytes 4718596
  59.1 1.1 %copy-start.16 = (f32[768,512]{1,0:T(8,128)}, f32[768,512]{1,0:T(8,128)S(1)}, u32[]{:S(2)}) copy-start(f32[768,512]{1,0:T(8,128)S(1)} %get-tuple-element.45.raw) | copy-start | bytes 4718596
  60.3 1.2 %copy-start.18 = (f32[768,512]{1,0:T(8,128)}, f32[768,512]{1,0:T(8,128)S(1)}, u32[]{:S(2)}) copy-start(f32[768,512]{1,0:T(8,128)S(1)} %get-tuple-element.47.gating) | copy-start | bytes 4718596
  61.4 0.9 copy-start.22
  77.5 1.4 %copy-start.13 = (f32[768,512]{1,0:T(8,128)S(1)}, f32[768,512]{1,0:T(8,128)}, u32[]{:S(2)}) copy-start(f32[768,512]{1,0:T(8,128)} %copy-done.12) | copy-start | bytes 4718596
  78.9 1.4 %copy-start.15 = (f32[768,512]{1,0:T(8,128)S(1)}, f32[768,512]{1,0:T(8,128)}, u32[]{:S(2)}) copy-start(f32[768,512]{1,0:T(8,128)} %copy-done.14) | copy-start | bytes 4718596
  80.3 1.1 %copy-start.21 = (bf16[768,512]{1,0:T(8,128)(2,1)S(1)}, bf16[768,512]{1,0:T(8,128)(2,1)}, u32[]{:S(2)}) copy-start(bf16[768,512]{1,0:T(8,128)(2,1)} %copy-done.20) | copy-start | bytes 2359300
  81.4 3.0 %copy-start.17 = (f32[768,512]{1,0:T(8,128)S(1)}, f32[768,512]{1,0:T(8,128)}, u32[]{:S(2)}) copy-start(f32[768,512]{1,0:T(8,128)} %copy-done.16) | copy-start | bytes 4718596
  81.4 3.0 %copy-start.19 = (f32[768,512]{1,0:T(8,128)S(1)}, f32[768,512]{1,0:T(8,128)}, u32[]{:S(2)}) copy-start(f32[768,512]{1,0:T(8,128)} %copy-done.18) | copy-start | bytes 4718596
  81.4 3.0 %copy-start.23 = (bf16[768,512]{1,0:T(8,128)(2,1)S(1)}, bf16[768,512]{1,0:T(8,128)(2,1)}, u32[]{:S(2)}) copy-start(bf16[768,512]{1,0:T(8,128)(2,1)} %copy-done.22) | copy-start | bytes 2359300
  82.6 3.7 %collective-permute-start = (bf16[768,512]{1,0:T(8,128)(2,1)S(1)}, bf16[768,512]{1,0:T(8,128)(2,1)S(1)}, u32[]{:S(2)}, u32[]{:S(2)}) collective-permute-start(bf16[768,512]{1,0:T(8,128)(2,1)S(1)} %finish.3), channel_id=1, source_target_pairs={{0,1},{1,0},{2,3},{3,2},{4,5},{5,4},{6,7},{7,6},{8,9},{9,8},{10,11... | collective-permute-start | bytes 2359304 | tf_op jit(solution)/shard_map/ppermute | solution.py:393

commit v2 on v1

v2 whole, which is shorter than its diff:
```python
import functools

import jax
import jax.numpy as jnp
from jax import lax
from jax.experimental import pallas as pl
from jax.experimental.pallas import tpu as pltpu
from jax.sharding import Mesh
from jax.sharding import PartitionSpec as P

BLOCK = 128
UNROLL = 3
EPSILON = 1e-06
LOG2E = 1.4426950408889634
Z, Y, X = ("sp_0", "sp_1", "sp_2")
SP = (Z, Y, X)
PLANE = (Y, X)
SP_TP = (Z, Y, X, "tp")
F32 = jnp.float32
BF16 = jnp.bfloat16


def mm(a, b, dims=((1,), (0,))):
    return lax.dot_general(a, b, (dims, ((), ())), preferred_element_type=F32)


def iota(shape, axis):
    return lax.broadcasted_iota(jnp.int32, shape, axis)


def params(limit_mib):
    return pltpu.CompilerParams(
        dimension_semantics=("arbitrary",), vmem_limit_bytes=limit_mib * 1024 * 1024
    )


def deal_matrix(plane, depth, transposed):
    rows = plane * depth
    dealt = iota((rows, rows), 1 if transposed else 0)
    natural = iota((rows, rows), 0 if transposed else 1)
    return ((dealt % depth) * plane + dealt // depth == natural).astype(BF16)


def log2_of_rest(gate):
    near = gate * (gate * (gate * (-LOG2E / 3) - LOG2E / 2) - LOG2E)
    return jnp.where(gate < 1e-3, near, jnp.log2(1.0 - gate))


def stretch_kernel(heads, plane, depth, unroll, gap_in, gain_in, query_in, logit_in, value_in,
                   gate_in, raw_out, reach_out, gating_out, send_out,
                   query, logit, value, gate, key_gates, cumuls, gap, gain, state, decay, pair, sems, small_sems):
    blocks = query.shape[0] // BLOCK
    sides = ((logit_in, logit), (value_in, value), (query_in, query), (gate_in, gate))

    def copies(i, first, last):
        rows = pl.ds(i * unroll * BLOCK, unroll * BLOCK)
        return [
            pltpu.make_async_copy(source.at[rows, :], target.at[rows, :], sems.at[n, i])
            for n, (source, target) in list(enumerate(sides))[first:last]
        ]

    small = [
        pltpu.make_async_copy(gap_in, gap, small_sems.at[0]),
        pltpu.make_async_copy(gain_in, gain, small_sems.at[1]),
    ]
    for copy in small:
        copy.start()
    for part in ((0, 1), (1, 4)):
        for i in range(blocks // unroll):
            for copy in copies(i, *part):
                copy.start()
    state[...] = jnp.zeros_like(state)
    decay[...] = jnp.ones_like(decay)
    causal = iota((BLOCK, BLOCK), 0) >= iota((BLOCK, BLOCK), 1)
    lower = causal.astype(BF16)
    lower2 = jnp.concatenate([lower, lower], axis=1)
    head_cols = [pl.ds(h * 128, 128) for h in range(heads)]
    for copy in small:
        copy.wait()

    def rows_of(block):
        return pl.ds(pl.multiple_of(block * BLOCK, BLOCK), BLOCK)

    def sum_logs(i, carry):
        for copy in copies(i, 0, 1):
            copy.wait()
        for b in range(unroll):
            rows = rows_of(i * unroll + b)
            highs, lows = [], []
            for cols in head_cols:
                key_gate = gap[:, cols] * jax.nn.sigmoid(-logit[rows, cols].astype(F32))
                key_gates[rows, cols] = key_gate
                log_forget = log2_of_rest(key_gate)
                highs.append(log_forget.astype(BF16))
                lows.append((log_forget - highs[-1].astype(F32)).astype(BF16))
            split = jnp.concatenate(
                [jnp.concatenate(highs, axis=1), jnp.concatenate(lows, axis=1)], axis=0
            )
            cumuls[rows, :] = mm(lower2, split)
        return carry

    lax.fori_loop(0, blocks // unroll, sum_logs, 0)

    def advance(i, carry):
        for copy in copies(i, 1, 4):
            copy.wait()
        for b in range(unroll):
            rows = rows_of(i * unroll + b)
            scores, inters, updates, decays = [], [], [], []
            for cols in head_cols:
                cumul = cumuls[rows, cols]
                grow = jnp.exp2(cumul)
                key = (key_gates[rows, cols] * jnp.exp2(-cumul)).astype(BF16)
                reader = jax.nn.silu(query[rows, cols].astype(F32)) * grow
                reach_out[rows, cols] = (reader * decay[:, cols]).astype(BF16)
                reader = reader.astype(BF16)
                scores.append(mm(reader, key, ((1,), (1,))))
                inters.append(mm(reader, state[:, cols].astype(BF16), ((1,), (1,))))
                updates.append(mm(value[rows, cols], key, ((0,), (0,))))
                decays.append(grow[BLOCK - 1 :, :])
            for h, cols in enumerate(head_cols):
                gating_out[rows, cols] = (
                    jax.nn.silu(gate[rows, cols].astype(F32)) * gain[:, cols]
                )
                score = jnp.where(causal, scores[h], 0.0).astype(BF16)
                raw_out[rows, cols] = mm(score, value[rows, cols]) + inters[h]
                state[:, cols] = decays[h] * (state[:, cols] + updates[h])
                decay[:, cols] = decay[:, cols] * decays[h]
        return carry

    lax.fori_loop(0, blocks // unroll, advance, 0)

    deal = deal_matrix(plane, depth, False)
    for h in range(heads):
        cols = pl.ds(h * 128, 128)
        dealt = mm(deal, state[:, cols].astype(BF16), ((1,), (1,)))
        send_out[:, h * depth : (h + 1) * depth, :] = (
            dealt.reshape(plane, depth, 128).astype(BF16)
        )
        whole = decay[:, cols]
        high = whole.astype(BF16).astype(F32)
        pair[h : h + 1, :] = high
        pair[heads + h : heads + h + 1, :] = whole - high
    tail = pair[...].astype(BF16)
    for p in range(plane):
        send_out[p, heads * depth :, :] = tail


SMEM_SPEC = pl.BlockSpec(memory_space=pltpu.SMEM)
VMEM_SPEC = pl.BlockSpec(memory_space=pltpu.VMEM)
HBM_SPEC = pl.BlockSpec(memory_space=pltpu.HBM)


def in_hbm(*arrays):
    return [pltpu.with_memory_space_constraint(array, pltpu.HBM) for array in arrays]


def stretch(gap, gain, query, logit, value, gate, heads, plane, depth, unroll):
    span, width = query.shape
    steps = span // BLOCK // unroll
    return pl.pallas_call(
        functools.partial(stretch_kernel, heads, plane, depth, unroll),
        in_specs=[HBM_SPEC] * 6,
        out_specs=[VMEM_SPEC] * 4,
        out_shape=[
            jax.ShapeDtypeStruct((span, width), F32),
            jax.ShapeDtypeStruct((span, width), BF16),
            jax.ShapeDtypeStruct((span, width), F32),
            jax.ShapeDtypeStruct((plane, heads * depth + 2 * heads, 128), BF16),
        ],
        scratch_shapes=[pltpu.VMEM((span, width), BF16)] * 4
        + [pltpu.VMEM((span, width), F32)] * 2
        + [
            pltpu.VMEM((1, width), F32),
            pltpu.VMEM((1, width), F32),
            pltpu.VMEM((128, width), F32),
            pltpu.VMEM((1, width), F32),
            pltpu.VMEM((2 * heads, 128), F32),
            pltpu.SemaphoreType.DMA((4, steps)),
            pltpu.SemaphoreType.DMA((2,)),
        ],
        compiler_params=pltpu.CompilerParams(vmem_limit_bytes=28 * 1024 * 1024),
        cost_estimate=pl.CostEstimate(flops=6_000_000_000, bytes_accessed=10_000_000, transcendentals=0),
        name="stretch",
    )(*in_hbm(gap, gain, query, logit, value, gate))


def decay_columns(place, received, heads, depth, plane):
    count = received.shape[0]
    picked = (iota((depth, 128), 1) == iota((depth, 128), 0) * plane + place).astype(BF16)
    parts = received[:, heads * depth :, :].reshape(count * 2 * heads, 128)
    columns = mm(picked, parts, ((1,), (1,)))
    lanes = columns.shape[1]
    return columns + pltpu.roll(columns, lanes - heads, 1)


def plane_kernel(heads, plane, depth, place, received, send_out, prefix_out, product_out):
    columns = decay_columns(place[0], received, heads, depth, plane)
    total = None
    states = [jnp.zeros((depth, 128), F32) for _ in range(heads)]
    products = [jnp.ones((depth, 128), F32) for _ in range(heads)]
    for s in range(plane):
        parts = received[s, heads * depth :, :].astype(F32)
        row_decay = parts + pltpu.roll(parts, heads, 0)
        total = row_decay if total is None else total * row_decay
        for h in range(heads):
            rows = slice(h * depth, (h + 1) * depth)
            prefix_out[s, rows, :] = states[h]
            product_out[s, rows, :] = products[h]
            lane = s * 2 * heads + h
            decay = jnp.broadcast_to(columns[:, lane : lane + 1], (depth, 128))
            states[h] = decay * states[h] + received[s, rows, :].astype(F32)
            products[h] = decay * products[h]
    high = total.astype(BF16).astype(F32)
    tail = jnp.where(iota(total.shape, 0) < heads, high, total - high).astype(BF16)
    for d in range(send_out.shape[0]):
        for h in range(heads):
            send_out[d, h * depth : (h + 1) * depth, :] = states[h].astype(BF16)
        send_out[d, heads * depth :, :] = tail


def plane_scan(place, received, heads, depth):
    plane, tall, _ = received.shape
    rows = heads * depth
    return pl.pallas_call(
        functools.partial(plane_kernel, heads, plane, depth),
        in_specs=[SMEM_SPEC, VMEM_SPEC],
        out_specs=[VMEM_SPEC] * 3,
        out_shape=[
            jax.ShapeDtypeStruct((depth, tall, 128), BF16),
            jax.ShapeDtypeStruct((plane, rows, 128), F32),
            jax.ShapeDtypeStruct((plane, rows, 128), F32),
        ],
        compiler_params=pltpu.CompilerParams(vmem_limit_bytes=8 * 1024 * 1024),
        cost_estimate=pl.CostEstimate(flops=100_000_000, bytes_accessed=1_000_000, transcendentals=0),
        name="plane_scan",
    )(place, received)


def depth_kernel(heads, plane, depth, place, received, prefix, product, first,
                 send_out, final_out, entering, final):
    columns = decay_columns(place[0], received, heads, depth, plane)
    states = [first[h, pl.ds(place[0], depth, stride=plane), :] for h in range(heads)]
    for s in range(depth):
        for h in range(heads):
            rows = slice(h * depth, (h + 1) * depth)
            entering[s, rows, :] = states[h]
            lane = s * 2 * heads + h
            decay = jnp.broadcast_to(columns[:, lane : lane + 1], (depth, 128))
            states[h] = decay * states[h] + received[s, rows, :].astype(F32)
    for h in range(heads):
        final[h] = states[h]
        final_out[h : h + 1, :] = final[h, pl.ds(place[1], 1), :]
    mine = entering[place[1]]
    for p in range(plane):
        send_out[p] = (prefix[p] + product[p] * mine).astype(BF16)


def depth_scan(place, received, prefix, product, first, heads):
    depth, tall, _ = received.shape
    plane, rows, _ = prefix.shape
    return pl.pallas_call(
        functools.partial(depth_kernel, heads, plane, depth),
        in_specs=[SMEM_SPEC] + [VMEM_SPEC] * 4,
        out_specs=[VMEM_SPEC] * 2,
        out_shape=[
            jax.ShapeDtypeStruct((plane, rows, 128), BF16),
            jax.ShapeDtypeStruct((heads, 128), F32),
        ],
        scratch_shapes=[
            pltpu.VMEM((depth, rows, 128), F32),
            pltpu.VMEM((heads, depth, 128), F32),
        ],
        compiler_params=pltpu.CompilerParams(vmem_limit_bytes=8 * 1024 * 1024),
        cost_estimate=pl.CostEstimate(flops=100_000_000, bytes_accessed=1_000_000, transcendentals=0),
        name="depth_scan",
    )(place, received, prefix, product, first)


def finish_kernel(heads, depth, half, incoming, raw, reach, gating, gated_out, state):
    plane = incoming.shape[0]

    @pl.when(pl.program_id(0) == 0)
    def _():
        collect = deal_matrix(plane, depth, True)
        for h in range(heads):
            part = incoming[:, h * depth : (h + 1) * depth, :].astype(F32)
            part = part.reshape(plane * depth, 128).astype(BF16)
            state[h] = mm(collect, part).astype(BF16)

    mean = jnp.full((128, 128), 1.0 / 128, BF16)
    for b in range(raw.shape[0] // BLOCK):
        rows = pl.ds(b * BLOCK, BLOCK)
        for h in range(heads):
            cols = pl.ds(h * 128, 128)
            value = raw[rows, cols] + mm(reach[rows, cols], state[h])
            mean_square = mm((value * value).astype(BF16), mean)
            gated_out[rows, cols] = (
                value * lax.rsqrt(mean_square + EPSILON) * gating[rows, cols]
            ).astype(BF16)


def finish(half, incoming, raw, reach, gating, heads, depth, rows):
    span, width = raw.shape
    steps = span // 2 // rows
    tall = pl.BlockSpec((rows, width), lambda i, w: (w[0] * steps + i, 0))
    return pl.pallas_call(
        functools.partial(finish_kernel, heads, depth),
        grid_spec=pltpu.PrefetchScalarGridSpec(
            num_scalar_prefetch=1,
            grid=(steps,),
            in_specs=[pl.BlockSpec(incoming.shape, lambda i, w: (0, 0, 0)), tall, tall, tall],
            out_specs=pl.BlockSpec((rows, width), lambda i, w: (i, 0)),
            scratch_shapes=[pltpu.VMEM((heads, 128, 128), BF16)],
        ),
        out_shape=jax.ShapeDtypeStruct((span // 2, width), BF16),
        compiler_params=params(12),
        cost_estimate=pl.CostEstimate(flops=2_000_000_000, bytes_accessed=4_000_000, transcendentals=0),
        name="finish",
    )(half, incoming, raw, reach, gating)


def project_kernel(mine, theirs, my_weight, their_weight, out):
    total = mm(mine[...], my_weight[...]) + mm(theirs[...], their_weight[...])
    out[...] = total.astype(BF16)


def project(mine, theirs, my_weight, their_weight, rows):
    total, inner = mine.shape
    width = my_weight.shape[1]
    left = pl.BlockSpec((rows, inner), lambda i: (i, 0))
    right = pl.BlockSpec((inner, width), lambda i: (0, 0))
    return pl.pallas_call(
        project_kernel,
        grid=(total // rows,),
        in_specs=[left, left, right, right],
        out_specs=pl.BlockSpec((rows, width), lambda i: (i, 0)),
        out_shape=jax.ShapeDtypeStruct((total, width), BF16),
        compiler_params=params(20),
        cost_estimate=pl.CostEstimate(flops=3_300_000_000, bytes_accessed=9_000_000, transcendentals=0),
        name="project",
    )(mine, theirs, my_weight, their_weight)


def per_device(
    queries, forget_logit, value_rows, out_gate, floor_gap, head_gain, state_in, out_weight
):
    heads = state_in.shape[0]
    plane = lax.axis_size(PLANE)
    depth = lax.axis_size(Z)
    place_plane = lax.axis_index(PLANE)
    place = jnp.stack([place_plane, lax.axis_index(Z)]).astype(jnp.int32)
    core = lax.axis_index("tp")
    other_half = (1 - core).reshape(1).astype(jnp.int32)
    my_half = core.reshape(1).astype(jnp.int32)
    swap = [(0, 1), (1, 0)]
    barrier = lax.optimization_barrier

    gap = floor_gap.reshape(1, -1)
    gain = head_gain.reshape(1, -1)
    gap, place, my_half, other_half = barrier((gap, place, my_half, other_half))

    *local, send = stretch(
        gap, gain, queries, forget_logit, value_rows, out_gate, heads, plane, depth, UNROLL
    )
    send, out_weight = barrier((send, out_weight))
    their_weight = lax.ppermute(out_weight, "tp", swap)
    received = lax.all_to_all(send, PLANE, 0, 0, tiled=True)

    send, prefix, product = plane_scan(place, received, heads, depth)
    received = lax.all_to_all(send, Z, 0, 0, tiled=True)
    send, state_out = depth_scan(place, received, prefix, product, state_in, heads)
    incoming = lax.all_to_all(send, PLANE, 0, 0, tiled=True)

    far_gated = finish(other_half, incoming, *local, heads, depth, 384)
    theirs = lax.ppermute(far_gated, "tp", swap)
    mine = finish(my_half, incoming, *local, heads, depth, 384)
    projected = project(mine, theirs, out_weight, their_weight, 256)
    return (projected, state_out)


def solution(mesh):
    torus = Mesh(mesh.devices.reshape(8, 4, 4, mesh.shape["tp"]), (Z, Y, X, "tp"))
    placed = (
        P(SP, "tp"),
        P(SP, "tp"),
        P(SP, "tp"),
        P(SP, "tp"),
        P("tp"),
        P("tp"),
        P("tp", None, None),
        P("tp", None),
    )
    return jax.shard_map(
        per_device,
        mesh=torus,
        in_specs=placed,
        out_specs=(P(SP_TP, None), P("tp", SP)),
        check_vma=False,
    )
```

time: 95.3 us -> 65.5 us (0.69)
  local copies, waits for them, and re-layouts: 35.9 us -> 0.01 us
  blocking collectives: 13.6 us -> 37.1 us
  starting transfers between devices: 18.6 us -> 7.51 us
  Pallas kernels: 24.7 us -> 19.2 us
    unnamed x66 -> x4, local copies, waits for them, and re-layouts: 35.9 us -> 0.01 us
    all_to_all x0 -> x2, blocking collectives: none -> 27.6 us  [the longest x1 15.4 us: per_device(): received = lax.all_to_all(send, Z, 0, 0, tiled=True)]
    all_to_all x2 -> x0, starting transfers between devices: 15.8 us -> none  [the longest x1 8.18 us: per_device(): received = lax.all_to_all(send, Z, 0, 0, tiled=True)]
    pallas_call x8 -> x6, Pallas kernels: 24.7 us -> 19.2 us  [the longest x1 9.55 us: stretch(): pl.pallas_call(functools.partial(stretch_kernel, heads, plane, depth, unr...]
    all_to_all x1, blocking collectives: 13.6 us -> 9.47 us  [per_device(): incoming = lax.all_to_all(send, PLANE, 0, 0, tiled=True)]
    ppermute x1, starting transfers between devices: 1.82 us -> 4.22 us  [per_device(): theirs = lax.ppermute(far_gated, 'tp', swap)]
    ppermute x1, starting transfers between devices: 1.04 us -> 3.29 us  [per_device(): their_weight = lax.ppermute(out_weight, 'tp', swap)]
  transfers between devices with their start and end apart: 4 -> 2, of which waited for: 1 -> 1; matrix products, arithmetic and copies ran while one was open for 0% -> 0% of each run, Pallas kernels for 11% -> 7%
where the time goes in v2:
time: 65.5 us; the launch traced here: 65.3 us
  blocking collectives  37.1 us (57%)
  Pallas kernels  19.2 us (29%)
  starting transfers between devices  7.51 us (11%)
  waiting for transfers between devices  0.77 us (1%)
  between operations  0.68 us (1%)
    all_to_all x1, blocking collectives, per_device(): received = lax.all_to_all(send, Z, 0, 0, tiled=True)  15.4 us
    all_to_all x1, blocking collectives, per_device(): received = lax.all_to_all(send, PLANE, 0, 0, tiled=True)  12.3 us
    pallas_call x1, Pallas kernels, stretch(): pl.pallas_call(functools.partial(stretch_kernel, heads, plane, depth, unr...  9.55 us
    all_to_all x1, blocking collectives, per_device(): incoming = lax.all_to_all(send, PLANE, 0, 0, tiled=True)  9.47 us
    pallas_call x1, Pallas kernels, project(): pl.pallas_call(project_kernel, grid=(total // rows,), in_specs=[left, lef...  4.83 us
    ppermute x1, starting transfers between devices, per_device(): theirs = lax.ppermute(far_gated, 'tp', swap)  4.22 us
    ppermute x1, starting transfers between devices, per_device(): their_weight = lax.ppermute(out_weight, 'tp', swap)  3.29 us
    pallas_call x2, Pallas kernels, finish(): pl.pallas_call(functools.partial(finish_kernel, heads, depth), grid_spec=...  2.27 us
  transfers between devices with their start and end apart: 2, of which 1 were waited for; matrix products, arithmetic and copies ran while one was open for 0% of the time, Pallas kernels for 7%

profile of v2, /device:TPU:1, one launch (start us, length us, event | category | flops | bytes accessed | tf_op | source)
XLA Modules:
  0.0 65.3 jit_solution(17192076182678037621)
XLA Ops:
  0.6 0.1 pad_add_fusion.place
  0.7 0.0 copy-start.1
  0.7 0.0 copy-start
  0.7 9.5 %stretch.1 = (f32[1536,512]{1,0:T(8,128)S(1)}, bf16[1536,512]{1,0:T(8,128)(2,1)S(1)}, f32[1536,512]{1,0:T(8,128)S(1)}, bf16[16,40,128]{2,1,0:T(8,128)(2,1)S(1)}) custom-call(f32[1,512]{1,0:T(1,128)} %bitcast.6, f32[1,512]{1,0:T(1,128)} %bitcast.7, bf16[1536,512]{1,0:T(8,128)(2,1)} %query_in.1, bf16[1536,512]{1,0:T(8,128)(2,1)} %logit_in.1, ...), custom_call_target="tpu_custom_call" | custom-call | flops 6000000000 | bytes 10000000 | tf_op jit(solution)/shard_map/stretch/pallas_call | solution.py:161
  10.3 0.0 copy-done.1
  10.3 3.3 %collective-permute-start.1 = (bf16[512,2048]{1,0:T(8,128)(2,1)S(1)}, bf16[512,2048]{1,0:T(8,128)(2,1)S(1)}, u32[]{:S(2)}, u32[]{:S(2)}) collective-permute-start(bf16[512,2048]{1,0:T(8,128)(2,1)S(1)} %copy-done.1), channel_id=1, source_target_pairs={{0,1},{1,0},{2,3},{3,2},{4,5},{5,4},{6,7},{7,6},{8,9},{9,8},{10,11... | collective-permute-start | bytes 6291464 | tf_op jit(solution)/shard_map/ppermute | solution.py:367
  13.6 12.3 %all_to_all.15.received = bf16[16,40,128]{2,1,0:T(8,128)(2,1)S(1)} all-to-all(bf16[16,40,128]{2,1,0:T(8,128)(2,1)S(1)} %get-tuple-element.21), channel_id=1, replica_groups=mesh['sp_0'=8,'sp_1'=4,'sp_2'=4,'tp'=2] {'sp_1','sp_2'}, dimensions={0} | all-to-all | bytes 327680 | tf_op jit(solution)/shard_map/all_to_all | solution.py:368
  25.8 0.9 %plane_scan.1 = (bf16[8,40,128]{2,1,0:T(8,128)(2,1)S(1)}, f32[16,32,128]{2,1,0:T(8,128)S(1)}, f32[16,32,128]{2,1,0:T(8,128)S(1)}) custom-call(s32[2]{0:T(128)S(1)} %pad_add_fusion.place, bf16[16,40,128]{2,1,0:T(8,128)(2,1)S(1)} %all_to_all.15.received), custom_call_target="tpu_custom_call" | custom-call | flops 100000000 | bytes 1000000 | tf_op jit(solution)/shard_map/plane_scan/pallas_call | solution.py:225
  26.8 15.4 %all_to_all.16.received = bf16[8,40,128]{2,1,0:T(8,128)(2,1)S(1)} all-to-all(bf16[8,40,128]{2,1,0:T(8,128)(2,1)S(1)} %get-tuple-element.22), channel_id=1, replica_groups=mesh['sp_0'=8,'sp_1'=4,'sp_2'=4,'tp'=2] {'sp_0'}, dimensions={0} | all-to-all | bytes 163840 | tf_op jit(solution)/shard_map/all_to_all | solution.py:371
  42.2 0.0 copy-done
  42.2 1.6 %depth_scan.1 = (bf16[16,32,128]{2,1,0:T(8,128)(2,1)S(1)}, f32[4,128]{1,0:T(4,128)}) custom-call(s32[2]{0:T(128)S(1)} %pad_add_fusion.place, bf16[8,40,128]{2,1,0:T(8,128)(2,1)S(1)} %all_to_all.16.received, f32[16,32,128]{2,1,0:T(8,128)S(1)} %get-tuple-element.23.prefix, f32[16,32,128]{2,1,0:T(8,128)S(1)} %get-tuple-element.24.product, ...), custom_call_target="tpu_custom_call" | custom-call | flops 100000000 | bytes 1000000 | tf_op jit(solution)/shard_map/depth_scan/pallas_call | solution.py:262
  43.7 9.5 %all_to_all.17.incoming = bf16[16,32,128]{2,1,0:T(8,128)(2,1)S(1)} all-to-all(bf16[16,32,128]{2,1,0:T(8,128)(2,1)S(1)} %get-tuple-element.25), channel_id=1, replica_groups=mesh['sp_0'=8,'sp_1'=4,'sp_2'=4,'tp'=2] {'sp_1','sp_2'}, dimensions={0} | all-to-all | bytes 262144 | tf_op jit(solution)/shard_map/all_to_all | solution.py:373
  53.2 1.1 %finish.3 = bf16[768,512]{1,0:T(8,128)(2,1)S(1)} custom-call(s32[1]{0:T(128)} %bitcast.4.half, bf16[16,32,128]{2,1,0:T(8,128)(2,1)S(1)} %all_to_all.17.incoming, f32[1536,512]{1,0:T(8,128)S(1)} %get-tuple-element.26.raw, bf16[1536,512]{1,0:T(8,128)(2,1)S(1)} %get-tuple-element.27.reach, f32[1536,512]{1,0:T(8,128)S(1)} %get-tuple-element.28.gating), custom_call_target="tpu_custom_call" | custom-call | flops 2000000000 | bytes 4000000 | tf_op jit(solution)/shard_map/finish/pallas_call | solution.py:307
  54.4 4.2 %collective-permute-start = (bf16[768,512]{1,0:T(8,128)(2,1)S(1)}, bf16[768,512]{1,0:T(8,128)(2,1)S(1)}, u32[]{:S(2)}, u32[]{:S(2)}) collective-permute-start(bf16[768,512]{1,0:T(8,128)(2,1)S(1)} %finish.3), channel_id=1, source_target_pairs={{0,1},{1,0},{2,3},{3,2},{4,5},{5,4},{6,7},{7,6},{8,9},{9,8},{10,11... | collective-permute-start | bytes 2359304 | tf_op jit(solution)/shard_map/ppermute | solution.py:376
  58.6 1.1 %finish.2.mine = bf16[768,512]{1,0:T(8,128)(2,1)S(1)} custom-call(s32[1]{0:T(128)} %bitcast.3.half, bf16[16,32,128]{2,1,0:T(8,128)(2,1)S(1)} %all_to_all.17.incoming, f32[1536,512]{1,0:T(8,128)S(1)} %get-tuple-element.26.raw, bf16[1536,512]{1,0:T(8,128)(2,1)S(1)} %get-tuple-element.27.reach, f32[1536,512]{1,0:T(8,128)S(1)} %get-tuple-element.28.gating), custom_call_target="tpu_custom_call" | custom-call | flops 2000000000 | bytes 4000000 | tf_op jit(solution)/shard_map/finish/pallas_call | solution.py:307
  59.7 0.8 %collective-permute-done.theirs = bf16[768,512]{1,0:T(8,128)(2,1)S(1)} collective-permute-done((bf16[768,512]{1,0:T(8,128)(2,1)S(1)}, bf16[768,512]{1,0:T(8,128)(2,1)S(1)}, u32[]{:S(2)}, u32[]{:S(2)}) %collective-permute-start) | collective-permute-done | bytes 786464 | tf_op jit(solution)/shard_map/ppermute | solution.py:376
  60.5 0.0 collective-permute-done.1.their_weight
  60.5 4.8 %project.1 = bf16[768,2048]{1,0:T(8,128)(2,1)} custom-call(bf16[768,512]{1,0:T(8,128)(2,1)S(1)} %finish.2.mine, bf16[768,512]{1,0:T(8,128)(2,1)S(1)} %collective-permute-done.theirs, bf16[512,2048]{1,0:T(8,128)(2,1)S(1)} %copy-done.1, bf16[512,2048]{1,0:T(8,128)(2,1)S(1)} %collective-permute-done.1.their_weight), custom_call_target="tpu_custom_call" | custom-call | flops 3300000000 | bytes 9000000 | tf_op jit(solution)/shard_map/project/pallas_call | solution.py:333
Async XLA Ops:
  0.7 9.6 %copy-start.1 = (bf16[512,2048]{1,0:T(8,128)(2,1)S(1)}, bf16[512,2048]{1,0:T(8,128)(2,1)}, u32[]{:S(2)}) copy-start(bf16[512,2048]{1,0:T(8,128)(2,1)} %my_weight) | copy-start | bytes 6291460
  0.7 41.4 %copy-start = (f32[4,128,128]{2,1,0:T(8,128)S(1)}, f32[4,128,128]{2,1,0:T(8,128)}, u32[]{:S(2)}) copy-start(f32[4,128,128]{2,1,0:T(8,128)} %first.1) | copy-start | bytes 786436
  10.3 50.2 %collective-permute-start.1 = (bf16[512,2048]{1,0:T(8,128)(2,1)S(1)}, bf16[512,2048]{1,0:T(8,128)(2,1)S(1)}, u32[]{:S(2)}, u32[]{:S(2)}) collective-permute-start(bf16[512,2048]{1,0:T(8,128)(2,1)S(1)} %copy-done.1), channel_id=1, source_target_pairs={{0,1},{1,0},{2,3},{3,2},{4,5},{5,4},{6,7},{7,6},{8,9},{9,8},{10,11... | collective-permute-start | bytes 6291464 | tf_op jit(solution)/shard_map/ppermute | solution.py:367
  54.4 6.1 %collective-permute-start = (bf16[768,512]{1,0:T(8,128)(2,1)S(1)}, bf16[768,512]{1,0:T(8,128)(2,1)S(1)}, u32[]{:S(2)}, u32[]{:S(2)}) collective-permute-start(bf16[768,512]{1,0:T(8,128)(2,1)S(1)} %finish.3), channel_id=1, source_target_pairs={{0,1},{1,0},{2,3},{3,2},{4,5},{5,4},{6,7},{7,6},{8,9},{9,8},{10,11... | collective-permute-start | bytes 2359304 | tf_op jit(solution)/shard_map/ppermute | solution.py:376

commit v3 on v2

--- a/solution.py
+++ b/solution.py
@@ -9,7 +9,7 @@
 from jax.sharding import PartitionSpec as P
 
 BLOCK = 128
-UNROLL = 3
+UNROLL = 4
 EPSILON = 1e-06
 LOG2E = 1.4426950408889634
 Z, Y, X = ("sp_0", "sp_1", "sp_2")
@@ -50,14 +50,15 @@
                    gate_in, raw_out, reach_out, gating_out, send_out,
                    query, logit, value, gate, key_gates, cumuls, gap, gain, state, decay, pair, sems, small_sems):
     blocks = query.shape[0] // BLOCK
-    sides = ((logit_in, logit), (value_in, value), (query_in, query), (gate_in, gate))
-
-    def copies(i, first, last):
+    sides = ((value_in, value), (query_in, query), (gate_in, gate))
+    rest = [
+        pltpu.make_async_copy(source, target, small_sems.at[2 + n])
+        for n, (source, target) in enumerate(sides)
+    ]
+
+    def logits(i):
         rows = pl.ds(i * unroll * BLOCK, unroll * BLOCK)
-        return [
-            pltpu.make_async_copy(source.at[rows, :], target.at[rows, :], sems.at[n, i])
-            for n, (source, target) in list(enumerate(sides))[first:last]
-        ]
+        return pltpu.make_async_copy(logit_in.at[rows, :], logit.at[rows, :], sems.at[i])
 
     small = [
         pltpu.make_async_copy(gap_in, gap, small_sems.at[0]),
@@ -65,10 +66,10 @@
     ]
     for copy in small:
         copy.start()
-    for part in ((0, 1), (1, 4)):
-        for i in range(blocks // unroll):
-            for copy in copies(i, *part):
-                copy.start()
+    for i in range(blocks // unroll):
+        logits(i).start()
+    for copy in rest:
+        copy.start()
     state[...] = jnp.zeros_like(state)
     decay[...] = jnp.ones_like(decay)
     causal = iota((BLOCK, BLOCK), 0) >= iota((BLOCK, BLOCK), 1)
@@ -82,8 +83,7 @@
         return pl.ds(pl.multiple_of(block * BLOCK, BLOCK), BLOCK)
 
     def sum_logs(i, carry):
-        for copy in copies(i, 0, 1):
-            copy.wait()
+        logits(i).wait()
         for b in range(unroll):
             rows = rows_of(i * unroll + b)
             highs, lows = [], []
@@ -101,9 +101,10 @@
 
     lax.fori_loop(0, blocks // unroll, sum_logs, 0)
 
+    for copy in rest:
+        copy.wait()
+
     def advance(i, carry):
-        for copy in copies(i, 1, 4):
-            copy.wait()
         for b in range(unroll):
             rows = rows_of(i * unroll + b)
             scores, inters, updates, decays = [], [], [], []
@@ -114,8 +115,10 @@
                 reader = jax.nn.silu(query[rows, cols].astype(F32)) * grow
                 reach_out[rows, cols] = (reader * decay[:, cols]).astype(BF16)
                 reader = reader.astype(BF16)
-                scores.append(mm(reader, key, ((1,), (1,))))
-                inters.append(mm(reader, state[:, cols].astype(BF16), ((1,), (1,))))
+                both = jnp.concatenate([key, state[:, cols].astype(BF16)], axis=0)
+                both = mm(reader, both, ((1,), (1,)))
+                scores.append(both[:, :BLOCK])
+                inters.append(both[:, BLOCK:])
                 updates.append(mm(value[rows, cols], key, ((0,), (0,))))
                 decays.append(grow[BLOCK - 1 :, :])
             for h, cols in enumerate(head_cols):
@@ -176,8 +179,8 @@
             pltpu.VMEM((128, width), F32),
             pltpu.VMEM((1, width), F32),
             pltpu.VMEM((2 * heads, 128), F32),
-            pltpu.SemaphoreType.DMA((4, steps)),
-            pltpu.SemaphoreType.DMA((2,)),
+            pltpu.SemaphoreType.DMA((steps,)),
+            pltpu.SemaphoreType.DMA((5,)),
         ],
         compiler_params=pltpu.CompilerParams(vmem_limit_bytes=28 * 1024 * 1024),
         cost_estimate=pl.CostEstimate(flops=6_000_000_000, bytes_accessed=10_000_000, transcendentals=0),
@@ -277,69 +280,119 @@
     )(place, received, prefix, product, first)
 
 
-def finish_kernel(heads, depth, half, incoming, raw, reach, gating, gated_out, state):
+def gather_state(heads, depth, incoming, state):
     plane = incoming.shape[0]
-
+    collect = deal_matrix(plane, depth, True)
+    for h in range(heads):
+        part = incoming[:, h * depth : (h + 1) * depth, :].astype(F32)
+        part = part.reshape(plane * depth, 128).astype(BF16)
+        state[h] = mm(collect, part).astype(BF16)
+
+
+def gated_rows(heads, rows, raw, reach, gating, state, gated_out):
+    for h in range(heads):
+        cols = pl.ds(h * 128, 128)
+        value = raw[rows, cols] + mm(reach[rows, cols], state[h])
+        mean_square = jnp.mean(value * value, axis=-1, keepdims=True)
+        gated_out[rows, cols] = (
+            value * lax.rsqrt(mean_square + EPSILON) * gating[rows, cols]
+        ).astype(BF16)
+
+
+def far_kernel(heads, depth, half, incoming, raw, reach, gating, gated_out, state):
     @pl.when(pl.program_id(0) == 0)
     def _():
-        collect = deal_matrix(plane, depth, True)
-        for h in range(heads):
-            part = incoming[:, h * depth : (h + 1) * depth, :].astype(F32)
-            part = part.reshape(plane * depth, 128).astype(BF16)
-            state[h] = mm(collect, part).astype(BF16)
-
-    mean = jnp.full((128, 128), 1.0 / 128, BF16)
+        gather_state(heads, depth, incoming, state)
+
     for b in range(raw.shape[0] // BLOCK):
-        rows = pl.ds(b * BLOCK, BLOCK)
-        for h in range(heads):
-            cols = pl.ds(h * 128, 128)
-            value = raw[rows, cols] + mm(reach[rows, cols], state[h])
-            mean_square = mm((value * value).astype(BF16), mean)
-            gated_out[rows, cols] = (
-                value * lax.rsqrt(mean_square + EPSILON) * gating[rows, cols]
-            ).astype(BF16)
-
-
-def finish(half, incoming, raw, reach, gating, heads, depth, rows):
+        gated_rows(heads, pl.ds(b * BLOCK, BLOCK), raw, reach, gating, state, gated_out)
+
+
+def near_kernel(heads, half, state, raw, reach, gating, weight, partial_out, gated):
+    for b in range(raw.shape[0] // BLOCK):
+        gated_rows(heads, pl.ds(b * BLOCK, BLOCK), raw, reach, gating, state, gated)
+    partial_out[...] = mm(gated[...], weight[...])
+
+
+def far_rows(half, incoming, raw, reach, gating, heads, depth, rows):
     span, width = raw.shape
     steps = span // 2 // rows
     tall = pl.BlockSpec((rows, width), lambda i, w: (w[0] * steps + i, 0))
     return pl.pallas_call(
-        functools.partial(finish_kernel, heads, depth),
+        functools.partial(far_kernel, heads, depth),
         grid_spec=pltpu.PrefetchScalarGridSpec(
             num_scalar_prefetch=1,
             grid=(steps,),
             in_specs=[pl.BlockSpec(incoming.shape, lambda i, w: (0, 0, 0)), tall, tall, tall],
-            out_specs=pl.BlockSpec((rows, width), lambda i, w: (i, 0)),
-            scratch_shapes=[pltpu.VMEM((heads, 128, 128), BF16)],
+            out_specs=[
+                pl.BlockSpec((rows, width), lambda i, w: (i, 0)),
+                pl.BlockSpec((heads, 128, 128), lambda i, w: (0, 0, 0)),
+            ],
         ),
-        out_shape=jax.ShapeDtypeStruct((span // 2, width), BF16),
+        out_shape=[
+            jax.ShapeDtypeStruct((span // 2, width), BF16),
+            jax.ShapeDtypeStruct((heads, 128, 128), BF16),
+        ],
         compiler_params=params(12),
         cost_estimate=pl.CostEstimate(flops=2_000_000_000, bytes_accessed=4_000_000, transcendentals=0),
-        name="finish",
+        name="far_rows",
     )(half, incoming, raw, reach, gating)
 
 
-def project_kernel(mine, theirs, my_weight, their_weight, out):
-    total = mm(mine[...], my_weight[...]) + mm(theirs[...], their_weight[...])
-    out[...] = total.astype(BF16)
-
-
-def project(mine, theirs, my_weight, their_weight, rows):
-    total, inner = mine.shape
-    width = my_weight.shape[1]
-    left = pl.BlockSpec((rows, inner), lambda i: (i, 0))
-    right = pl.BlockSpec((inner, width), lambda i: (0, 0))
+def near_rows(half, state, raw, reach, gating, weight, heads, rows):
+    span, width = raw.shape
+    inner, out_width = weight.shape
+    steps = span // 2 // rows
+    tall = pl.BlockSpec((rows, width), lambda i, w: (w[0] * steps + i, 0))
+    return pl.pallas_call(
+        functools.partial(near_kernel, heads),
+        grid_spec=pltpu.PrefetchScalarGridSpec(
+            num_scalar_prefetch=1,
+            grid=(steps,),
+            in_specs=[
+                pl.BlockSpec(state.shape, lambda i, w: (0, 0, 0)),
+                tall,
+                tall,
+                tall,
+                pl.BlockSpec((inner, out_width), lambda i, w: (0, 0)),
+            ],
+            out_specs=pl.BlockSpec((rows, out_width), lambda i, w: (i, 0)),
+            scratch_shapes=[pltpu.VMEM((rows, width), BF16)],
+        ),
+        out_shape=jax.ShapeDtypeStruct((span // 2, out_width), F32),
+        compiler_params=params(20),
+        cost_estimate=pl.CostEstimate(flops=4_000_000_000, bytes_accessed=4_000_000, transcendentals=0),
+        name="near_rows",
+    )(half, state, raw, reach, gating, weight)
+
+
+def project_kernel(partial, theirs, their_weight, final, out, final_out):
+    out[...] = (partial[...] + mm(theirs[...], their_weight[...])).astype(BF16)
+    final_out[...] = final[...]
+
+
+def project(partial, theirs, their_weight, final, rows):
+    total, width = partial.shape
+    inner = theirs.shape[1]
+    whole = pl.BlockSpec(final.shape, lambda i: (0, 0))
     return pl.pallas_call(
         project_kernel,
         grid=(total // rows,),
-        in_specs=[left, left, right, right],
-        out_specs=pl.BlockSpec((rows, width), lambda i: (i, 0)),
-        out_shape=jax.ShapeDtypeStruct((total, width), BF16),
+        in_specs=[
+            pl.BlockSpec((rows, width), lambda i: (i, 0)),
+            pl.BlockSpec((rows, inner), lambda i: (i, 0)),
+            pl.BlockSpec((inner, width), lambda i: (0, 0)),
+            whole,
+        ],
+        out_specs=[pl.BlockSpec((rows, width), lambda i: (i, 0)), whole],
+        out_shape=[
+            jax.ShapeDtypeStruct((total, width), BF16),
+            jax.ShapeDtypeStruct(final.shape, F32),
+        ],
         compiler_params=params(20),
         cost_estimate=pl.CostEstimate(flops=3_300_000_000, bytes_accessed=9_000_000, transcendentals=0),
         name="project",
-    )(mine, theirs, my_weight, their_weight)
+    )(partial, theirs, pltpu.with_memory_space_constraint(their_weight, pltpu.VMEM), final)
 
 
 def per_device(
@@ -369,13 +422,13 @@
 
     send, prefix, product = plane_scan(place, received, heads, depth)
     received = lax.all_to_all(send, Z, 0, 0, tiled=True)
-    send, state_out = depth_scan(place, received, prefix, product, state_in, heads)
+    send, final = depth_scan(place, received, prefix, product, state_in, heads)
     incoming = lax.all_to_all(send, PLANE, 0, 0, tiled=True)
 
-    far_gated = finish(other_half, incoming, *local, heads, depth, 384)
-    theirs = lax.ppermute(far_gated, "tp", swap)
-    mine = finish(my_half, incoming, *local, heads, depth, 384)
-    projected = project(mine, theirs, out_weight, their_weight, 256)
+    far, state = far_rows(other_half, incoming, *local, heads, depth, 384)
+    theirs = lax.ppermute(far, "tp", swap)
+    partial = near_rows(my_half, state, *local, out_weight, heads, 384)
+    projected, state_out = project(partial, theirs, their_weight, final, 256)
     return (projected, state_out)
 
 

time: 65.5 us -> 62.3 us (0.951)
  Pallas kernels: 19.2 us -> 16.7 us
  waiting for transfers between devices: 0.77 us -> 0.01 us
    pallas_call x1, Pallas kernels: 9.55 us -> 7.62 us  [stretch(): pl.pallas_call(functools.partial(stretch_kernel, heads, plane, depth, unr...]
    ppermute x1, waiting for transfers between devices: 0.77 us -> 0.01 us  [per_device(): theirs = lax.ppermute(far, 'tp', swap)]
  transfers between devices with their start and end apart: 2 -> 2, of which waited for: 1 -> 0; matrix products, arithmetic and copies ran while one was open for 0% -> 0% of each run, Pallas kernels for 7% -> 9%
where the time goes in v3:
time: 62.3 us; the launch traced here: 62.1 us
  blocking collectives  37.1 us (60%)
  Pallas kernels  16.7 us (27%)
  starting transfers between devices  7.51 us (12%)
  between operations  0.7 us (1%)
    all_to_all x1, blocking collectives, per_device(): received = lax.all_to_all(send, Z, 0, 0, tiled=True)  15.4 us
    all_to_all x1, blocking collectives, per_device(): received = lax.all_to_all(send, PLANE, 0, 0, tiled=True)  12.3 us
    all_to_all x1, blocking collectives, per_device(): incoming = lax.all_to_all(send, PLANE, 0, 0, tiled=True)  9.48 us
    pallas_call x1, Pallas kernels, stretch(): pl.pallas_call(functools.partial(stretch_kernel, heads, plane, depth, unr...  7.62 us
    ppermute x1, starting transfers between devices, per_device(): theirs = lax.ppermute(far, 'tp', swap)  4.22 us
    pallas_call x1, Pallas kernels, project(): pl.pallas_call(project_kernel, grid=(total // rows,), in_specs=[pl.BlockS...  3.39 us
    ppermute x1, starting transfers between devices, per_device(): their_weight = lax.ppermute(out_weight, 'tp', swap)  3.29 us
    pallas_call x1, Pallas kernels, near_rows(): pl.pallas_call(functools.partial(near_kernel, heads), grid_spec=pltpu.Pre...  2.58 us
  transfers between devices with their start and end apart: 2, of which 0 were waited for; matrix products, arithmetic and copies ran while one was open for 0% of the time, Pallas kernels for 9%

profile of v3, /device:TPU:1, one launch (start us, length us, event | category | flops | bytes accessed | tf_op | source)
XLA Modules:
  0.0 62.1 jit_solution(428290867922038088)
XLA Ops:
  0.6 0.1 pad_add_fusion.place
  0.7 0.0 copy-start
  0.7 0.0 copy-start.1
  0.7 7.6 %stretch.1 = (f32[1536,512]{1,0:T(8,128)S(1)}, bf16[1536,512]{1,0:T(8,128)(2,1)S(1)}, f32[1536,512]{1,0:T(8,128)S(1)}, bf16[16,40,128]{2,1,0:T(8,128)(2,1)S(1)}) custom-call(f32[1,512]{1,0:T(1,128)} %bitcast.6, f32[1,512]{1,0:T(1,128)} %bitcast.7, bf16[1536,512]{1,0:T(8,128)(2,1)} %query_in.1, bf16[1536,512]{1,0:T(8,128)(2,1)} %logit_in.1, ...), custom_call_target="tpu_custom_call" | custom-call | flops 6000000000 | bytes 10000000 | tf_op jit(solution)/shard_map/stretch/pallas_call | solution.py:164
  8.3 0.0 copy-done
  8.4 3.3 %collective-permute-start.1 = (bf16[512,2048]{1,0:T(8,128)(2,1)S(1)}, bf16[512,2048]{1,0:T(8,128)(2,1)S(1)}, u32[]{:S(2)}, u32[]{:S(2)}) collective-permute-start(bf16[512,2048]{1,0:T(8,128)(2,1)S(1)} %copy-done), channel_id=1, source_target_pairs={{0,1},{1,0},{2,3},{3,2},{4,5},{5,4},{6,7},{7,6},{8,9},{9,8},{10,11... | collective-permute-start | bytes 6291464 | tf_op jit(solution)/shard_map/ppermute | solution.py:420
  11.6 12.3 %all_to_all.15.received = bf16[16,40,128]{2,1,0:T(8,128)(2,1)S(1)} all-to-all(bf16[16,40,128]{2,1,0:T(8,128)(2,1)S(1)} %get-tuple-element.24), channel_id=1, replica_groups=mesh['sp_0'=8,'sp_1'=4,'sp_2'=4,'tp'=2] {'sp_1','sp_2'}, dimensions={0} | all-to-all | bytes 327680 | tf_op jit(solution)/shard_map/all_to_all | solution.py:421
  23.9 0.9 %plane_scan.1 = (bf16[8,40,128]{2,1,0:T(8,128)(2,1)S(1)}, f32[16,32,128]{2,1,0:T(8,128)S(1)}, f32[16,32,128]{2,1,0:T(8,128)S(1)}) custom-call(s32[2]{0:T(128)S(1)} %pad_add_fusion.place, bf16[16,40,128]{2,1,0:T(8,128)(2,1)S(1)} %all_to_all.15.received), custom_call_target="tpu_custom_call" | custom-call | flops 100000000 | bytes 1000000 | tf_op jit(solution)/shard_map/plane_scan/pallas_call | solution.py:228
  24.8 15.4 %all_to_all.16.received = bf16[8,40,128]{2,1,0:T(8,128)(2,1)S(1)} all-to-all(bf16[8,40,128]{2,1,0:T(8,128)(2,1)S(1)} %get-tuple-element.25), channel_id=1, replica_groups=mesh['sp_0'=8,'sp_1'=4,'sp_2'=4,'tp'=2] {'sp_0'}, dimensions={0} | all-to-all | bytes 163840 | tf_op jit(solution)/shard_map/all_to_all | solution.py:424
  40.2 0.0 copy-done.1
  40.2 1.0 %depth_scan.1 = (bf16[16,32,128]{2,1,0:T(8,128)(2,1)S(1)}, f32[4,128]{1,0:T(4,128)S(1)}) custom-call(s32[2]{0:T(128)S(1)} %pad_add_fusion.place, bf16[8,40,128]{2,1,0:T(8,128)(2,1)S(1)} %all_to_all.16.received, f32[16,32,128]{2,1,0:T(8,128)S(1)} %get-tuple-element.26.prefix, f32[16,32,128]{2,1,0:T(8,128)S(1)} %get-tuple-element.27.product, ...), custom_call_target="tpu_custom_call" | custom-call | flops 100000000 | bytes 1000000 | tf_op jit(solution)/shard_map/depth_scan/pallas_call | solution.py:265
  41.3 9.5 %all_to_all.17.incoming = bf16[16,32,128]{2,1,0:T(8,128)(2,1)S(1)} all-to-all(bf16[16,32,128]{2,1,0:T(8,128)(2,1)S(1)} %get-tuple-element.28), channel_id=1, replica_groups=mesh['sp_0'=8,'sp_1'=4,'sp_2'=4,'tp'=2] {'sp_1','sp_2'}, dimensions={0} | all-to-all | bytes 262144 | tf_op jit(solution)/shard_map/all_to_all | solution.py:426
  50.7 1.1 %far_rows.1 = (bf16[768,512]{1,0:T(8,128)(2,1)S(1)}, bf16[4,128,128]{2,1,0:T(8,128)(2,1)S(1)}) custom-call(s32[1]{0:T(128)} %bitcast.4.half, bf16[16,32,128]{2,1,0:T(8,128)(2,1)S(1)} %all_to_all.17.incoming, f32[1536,512]{1,0:T(8,128)S(1)} %get-tuple-element.29.raw, bf16[1536,512]{1,0:T(8,128)(2,1)S(1)} %get-tuple-element.30.reach, ...), custom_call_target="tpu_custom_call" | custom-call | flops 2000000000 | bytes 4000000 | tf_op jit(solution)/shard_map/far_rows/pallas_call | solution.py:321
  51.9 4.2 %collective-permute-start = (bf16[768,512]{1,0:T(8,128)(2,1)S(1)}, bf16[768,512]{1,0:T(8,128)(2,1)S(1)}, u32[]{:S(2)}, u32[]{:S(2)}) collective-permute-start(bf16[768,512]{1,0:T(8,128)(2,1)S(1)} %get-tuple-element.34), channel_id=1, source_target_pairs={{0,1},{1,0},{2,3},{3,2},{4,5},{5,4},{6,7},{7,6},{8,9},{9,8},{10,11... | collective-permute-start | bytes 2359304 | tf_op jit(solution)/shard_map/ppermute | solution.py:429
  56.1 2.6 %near_rows.1.partial = f32[768,2048]{1,0:T(8,128)S(1)} custom-call(s32[1]{0:T(128)} %bitcast.3.half, bf16[4,128,128]{2,1,0:T(8,128)(2,1)S(1)} %get-tuple-element.32.state, f32[1536,512]{1,0:T(8,128)S(1)} %get-tuple-element.29.raw, bf16[1536,512]{1,0:T(8,128)(2,1)S(1)} %get-tuple-element.30.reach, f32[1536,512]{1,0:T(8,128)S(1)} %get-tuple-element.31.gating, ...), custom_call_target="tpu_custom_call" | custom-call | flops 4000000000 | bytes 4000000 | tf_op jit(solution)/shard_map/near_rows/pallas_call | solution.py:347
  58.7 0.0 collective-permute-done.theirs
  58.7 0.0 collective-permute-done.1.their_weight
  58.7 3.4 %project.1 = (bf16[768,2048]{1,0:T(8,128)(2,1)}, f32[4,128]{1,0:T(4,128)}) custom-call(f32[768,2048]{1,0:T(8,128)S(1)} %near_rows.1.partial, bf16[768,512]{1,0:T(8,128)(2,1)S(1)} %collective-permute-done.theirs, bf16[512,2048]{1,0:T(8,128)(2,1)S(1)} %collective-permute-done.1.their_weight, f32[4,128]{1,0:T(4,128)S(1)} %get-tuple-element.35.final), custom_call_target="tpu_custom_call" | custom-call | flops 3300000000 | bytes 9000000 | tf_op jit(solution)/shard_map/project/pallas_call | solution.py:378
Async XLA Ops:
  0.7 7.6 %copy-start = (bf16[512,2048]{1,0:T(8,128)(2,1)S(1)}, bf16[512,2048]{1,0:T(8,128)(2,1)}, u32[]{:S(2)}) copy-start(bf16[512,2048]{1,0:T(8,128)(2,1)} %weight) | copy-start | bytes 6291460
  0.7 39.5 %copy-start.1 = (f32[4,128,128]{2,1,0:T(8,128)S(1)}, f32[4,128,128]{2,1,0:T(8,128)}, u32[]{:S(2)}) copy-start(f32[4,128,128]{2,1,0:T(8,128)} %first.1) | copy-start | bytes 786436
  8.4 50.3 %collective-permute-start.1 = (bf16[512,2048]{1,0:T(8,128)(2,1)S(1)}, bf16[512,2048]{1,0:T(8,128)(2,1)S(1)}, u32[]{:S(2)}, u32[]{:S(2)}) collective-permute-start(bf16[512,2048]{1,0:T(8,128)(2,1)S(1)} %copy-done), channel_id=1, source_target_pairs={{0,1},{1,0},{2,3},{3,2},{4,5},{5,4},{6,7},{7,6},{8,9},{9,8},{10,11... | collective-permute-start | bytes 6291464 | tf_op jit(solution)/shard_map/ppermute | solution.py:420
  51.9 6.8 %collective-permute-start = (bf16[768,512]{1,0:T(8,128)(2,1)S(1)}, bf16[768,512]{1,0:T(8,128)(2,1)S(1)}, u32[]{:S(2)}, u32[]{:S(2)}) collective-permute-start(bf16[768,512]{1,0:T(8,128)(2,1)S(1)} %get-tuple-element.34), channel_id=1, source_target_pairs={{0,1},{1,0},{2,3},{3,2},{4,5},{5,4},{6,7},{7,6},{8,9},{9,8},{10,11... | collective-permute-start | bytes 2359304 | tf_op jit(solution)/shard_map/ppermute | solution.py:429

commit v4 on v3

v4 whole, which is shorter than its diff:
```python
import functools

import jax
import jax.numpy as jnp
from jax import lax
from jax.experimental import pallas as pl
from jax.experimental.pallas import tpu as pltpu
from jax.sharding import Mesh
from jax.sharding import PartitionSpec as P

BLOCK = 128
UNROLL = 4
EPSILON = 1e-06
LOG2E = 1.4426950408889634
Z, Y, X = ("sp_0", "sp_1", "sp_2")
SP = (Z, Y, X)
PLANE = (Y, X)
SP_TP = (Z, Y, X, "tp")
F32 = jnp.float32
BF16 = jnp.bfloat16


def mm(a, b, dims=((1,), (0,))):
    return lax.dot_general(a, b, (dims, ((), ())), preferred_element_type=F32)


def iota(shape, axis):
    return lax.broadcasted_iota(jnp.int32, shape, axis)


def params(limit_mib):
    return pltpu.CompilerParams(
        dimension_semantics=("arbitrary",), vmem_limit_bytes=limit_mib * 1024 * 1024
    )


def deal_matrix(plane, depth, transposed):
    rows = plane * depth
    dealt = iota((rows, rows), 1 if transposed else 0)
    natural = iota((rows, rows), 0 if transposed else 1)
    return ((dealt % depth) * plane + dealt // depth == natural).astype(BF16)


def log2_of_rest(gate):
    near = gate * (gate * (-LOG2E / 2) - LOG2E)
    return jnp.where(gate < 1e-3, near, jnp.log2(1.0 - gate))


def goes_early(depth):
    return lax.axis_index(Z) < depth * 3 // 8


def rows_of(block):
    return pl.ds(pl.multiple_of(block * BLOCK, BLOCK), BLOCK)


def read_block(rows, cols, query, gate, gain, cumul, offset, key, state):
    reader = jax.nn.silu(query[rows, cols].astype(F32)) * jnp.exp2(cumul)
    reach = (reader * offset).astype(BF16)
    both = mm(reader.astype(BF16), jnp.concatenate([key, state], axis=0), ((1,), (1,)))
    gating = jax.nn.silu(gate[rows, cols].astype(F32)) * gain[:, cols]
    return both, reach, gating


def finish_block(causal, both, values):
    scores = jnp.where(causal, both[:, :BLOCK], 0.0).astype(BF16)
    return mm(scores, values) + both[:, BLOCK:]


def stretch_kernel(heads, plane, depth, unroll, gap_in, gain_in, query_in, logit_in, value_in,
                   gate_in, raw_out, reach_out, gating_out, send_out, query, value, gate, cumuls,
                   keys, starts, offsets, gain, logit, key_gates, gap, state, decay, pair,
                   sems, small_sems):
    blocks = query.shape[0] // BLOCK
    sides = ((value_in, value), (query_in, query), (gate_in, gate))
    rest = [
        pltpu.make_async_copy(source, target, small_sems.at[2 + n])
        for n, (source, target) in enumerate(sides)
    ]

    def logits(i):
        rows = pl.ds(i * unroll * BLOCK, unroll * BLOCK)
        return pltpu.make_async_copy(logit_in.at[rows, :], logit.at[rows, :], sems.at[i])

    small = [
        pltpu.make_async_copy(gap_in, gap, small_sems.at[0]),
        pltpu.make_async_copy(gain_in, gain, small_sems.at[1]),
    ]
    for copy in small:
        copy.start()
    for i in range(blocks // unroll):
        logits(i).start()
    for copy in rest:
        copy.start()
    state[...] = jnp.zeros_like(state)
    decay[...] = jnp.ones_like(decay)
    causal = iota((BLOCK, BLOCK), 0) >= iota((BLOCK, BLOCK), 1)
    lower = causal.astype(BF16)
    lower2 = jnp.concatenate([lower, lower], axis=1)
    head_cols = [pl.ds(h * 128, 128) for h in range(heads)]
    for copy in small:
        copy.wait()

    half_gap = 0.5 * gap[...]

    def sum_logs(i, carry):
        logits(i).wait()
        for b in range(unroll):
            rows = rows_of(i * unroll + b)
            highs, lows = [], []
            for h, cols in enumerate(head_cols):
                key_gate = half_gap[:, h * 128 : (h + 1) * 128] * (1.0 - jnp.tanh(0.5 * logit[rows, cols].astype(F32)))
                key_gates[rows, cols] = key_gate
                log_forget = log2_of_rest(key_gate)
                highs.append(log_forget.astype(BF16))
                lows.append((log_forget - highs[-1].astype(F32)).astype(BF16))
            split = jnp.concatenate(
                [jnp.concatenate(highs, axis=1), jnp.concatenate(lows, axis=1)], axis=0
            )
            cumuls[rows, :] = mm(lower2, split)
        return carry

    lax.fori_loop(0, blocks // unroll, sum_logs, 0)
    rest[0].wait()

    def advance(whole, i, carry):
        for b in range(unroll):
            block = i * unroll + b
            rows = rows_of(block)
            boths, updates, decays = [], [], []
            for cols in head_cols:
                cumul = cumuls[rows, cols]
                key = (key_gates[rows, cols] * jnp.exp2(-cumul)).astype(BF16)
                start = state[:, cols].astype(BF16)
                if whole:
                    both, reach_out[rows, cols], gating_out[rows, cols] = read_block(
                        rows, cols, query, gate, gain, cumul, decay[:, cols], key, start
                    )
                    boths.append(both)
                else:
                    keys[rows, cols] = key
                    starts[block, :, cols] = start
                    offsets[block, :, cols] = decay[:, cols]
                updates.append(mm(value[rows, cols], key, ((0,), (0,))))
                decays.append(jnp.exp2(cumul[BLOCK - 1 :, :]))
            for h, cols in enumerate(head_cols):
                if whole:
                    raw_out[rows, cols] = finish_block(causal, boths[h], value[rows, cols])
                state[:, cols] = decays[h] * (state[:, cols] + updates[h])
                decay[:, cols] = decay[:, cols] * decays[h]
        return carry

    early = goes_early(depth)

    @pl.when(early)
    def _():
        for copy in rest[1:]:
            copy.wait()
        lax.fori_loop(0, blocks // unroll, functools.partial(advance, True), 0)

    @pl.when(jnp.logical_not(early))
    def _():
        lax.fori_loop(0, blocks // unroll, functools.partial(advance, False), 0)
        for copy in rest[1:]:
            copy.wait()

    deal = deal_matrix(plane, depth, False)
    for h in range(heads):
        cols = pl.ds(h * 128, 128)
        dealt = mm(deal, state[:, cols].astype(BF16), ((1,), (1,)))
        send_out[:, h * depth : (h + 1) * depth, :] = (
            dealt.reshape(plane, depth, 128).astype(BF16)
        )
        whole = decay[:, cols]
        high = whole.astype(BF16).astype(F32)
        pair[h : h + 1, :] = high
        pair[heads + h : heads + h + 1, :] = whole - high
    tail = pair[...].astype(BF16)
    for p in range(plane):
        send_out[p, heads * depth :, :] = tail


def late_outputs(heads, query, value, gate, cumuls, keys, starts, offsets, gain,
                 raw_out, reach_out, gating_out):
    blocks = query.shape[0] // BLOCK
    causal = iota((BLOCK, BLOCK), 0) >= iota((BLOCK, BLOCK), 1)
    head_cols = [pl.ds(h * 128, 128) for h in range(heads)]

    def step(i, carry):
        for b in range(UNROLL):
            block = i * UNROLL + b
            rows = rows_of(block)
            boths = []
            for cols in head_cols:
                both, reach_out[rows, cols], gating_out[rows, cols] = read_block(
                    rows, cols, query, gate, gain, cumuls[rows, cols], offsets[block, :, cols],
                    keys[rows, cols], starts[block, :, cols],
                )
                boths.append(both)
            for both, cols in zip(boths, head_cols):
                raw_out[rows, cols] = finish_block(causal, both, value[rows, cols])
        return carry

    lax.fori_loop(0, blocks // UNROLL, step, 0)


VMEM_SPEC = pl.BlockSpec(memory_space=pltpu.VMEM)
HBM_SPEC = pl.BlockSpec(memory_space=pltpu.HBM)


def in_hbm(*arrays):
    return [pltpu.with_memory_space_constraint(array, pltpu.HBM) for array in arrays]


def stretch(gap, gain, query, logit, value, gate, heads, plane, depth, unroll):
    span, width = query.shape
    steps = span // BLOCK // unroll
    narrow = jax.ShapeDtypeStruct((span, width), BF16)
    wide = jax.ShapeDtypeStruct((span, width), F32)
    results = pl.pallas_call(
        functools.partial(stretch_kernel, heads, plane, depth, unroll),
        in_specs=[HBM_SPEC] * 6,
        out_specs=[VMEM_SPEC] * 12,
        out_shape=[
            wide,
            narrow,
            wide,
            jax.ShapeDtypeStruct((plane, heads * depth + 2 * heads, 128), BF16),
            narrow,
            narrow,
            narrow,
            wide,
            narrow,
            jax.ShapeDtypeStruct((span // BLOCK, 128, width), BF16),
            jax.ShapeDtypeStruct((span // BLOCK, 1, width), F32),
            jax.ShapeDtypeStruct((1, width), F32),
        ],
        scratch_shapes=[
            pltpu.VMEM((span, width), BF16),
            pltpu.VMEM((span, width), F32),
            pltpu.VMEM((1, width), F32),
            pltpu.VMEM((128, width), F32),
            pltpu.VMEM((1, width), F32),
            pltpu.VMEM((2 * heads, 128), F32),
            pltpu.SemaphoreType.DMA((steps,)),
            pltpu.SemaphoreType.DMA((5,)),
        ],
        compiler_params=pltpu.CompilerParams(vmem_limit_bytes=34 * 1024 * 1024),
        cost_estimate=pl.CostEstimate(flops=6_000_000_000, bytes_accessed=10_000_000, transcendentals=0),
        name="stretch",
    )(*in_hbm(gap, gain, query, logit, value, gate))
    return results[:3], results[3], results[4:]


def decay_columns(place, received, heads, depth, plane):
    count = received.shape[0]
    picked = (iota((depth, 128), 1) == iota((depth, 128), 0) * plane + place).astype(BF16)
    parts = received[:, heads * depth :, :].reshape(count * 2 * heads, 128)
    columns = mm(picked, parts, ((1,), (1,)))
    lanes = columns.shape[1]
    return columns + pltpu.roll(columns, lanes - heads, 1)


def plane_kernel(heads, plane, depth, received, send_out, prefix_out, product_out):
    columns = decay_columns(lax.axis_index(PLANE), received, heads, depth, plane)
    total = None
    states = [jnp.zeros((depth, 128), F32) for _ in range(heads)]
    products = [jnp.ones((depth, 128), F32) for _ in range(heads)]
    for s in range(plane):
        parts = received[s, heads * depth :, :].astype(F32)
        row_decay = parts + pltpu.roll(parts, heads, 0)
        total = row_decay if total is None else total * row_decay
        for h in range(heads):
            rows = slice(h * depth, (h + 1) * depth)
            prefix_out[s, rows, :] = states[h]
            product_out[s, rows, :] = products[h]
            lane = s * 2 * heads + h
            decay = jnp.broadcast_to(columns[:, lane : lane + 1], (depth, 128))
            states[h] = decay * states[h] + received[s, rows, :].astype(F32)
            products[h] = decay * products[h]
    high = total.astype(BF16).astype(F32)
    tail = jnp.where(iota(total.shape, 0) < heads, high, total - high).astype(BF16)
    for d in range(send_out.shape[0]):
        for h in range(heads):
            send_out[d, h * depth : (h + 1) * depth, :] = states[h].astype(BF16)
        send_out[d, heads * depth :, :] = tail


def plane_scan(received, heads, depth):
    plane, tall, _ = received.shape
    rows = heads * depth
    return pl.pallas_call(
        functools.partial(plane_kernel, heads, plane, depth),
        in_specs=[VMEM_SPEC],
        out_specs=[VMEM_SPEC] * 3,
        out_shape=[
            jax.ShapeDtypeStruct((depth, tall, 128), BF16),
            jax.ShapeDtypeStruct((plane, rows, 128), F32),
            jax.ShapeDtypeStruct((plane, rows, 128), F32),
        ],
        compiler_params=pltpu.CompilerParams(vmem_limit_bytes=8 * 1024 * 1024),
        cost_estimate=pl.CostEstimate(flops=100_000_000, bytes_accessed=1_000_000, transcendentals=0),
        name="plane_scan",
    )(received)


def depth_kernel(heads, plane, depth, received, prefix, product, first, query, value, gate,
                 cumuls, keys, starts, offsets, gain, raw_in, reach_in, gating_in,
                 send_out, final_out, raw_out, reach_out, gating_out, entering, final):
    columns = decay_columns(lax.axis_index(PLANE), received, heads, depth, plane)
    states = [first[h, pl.ds(lax.axis_index(PLANE), depth, stride=plane), :] for h in range(heads)]
    for s in range(depth):
        for h in range(heads):
            rows = slice(h * depth, (h + 1) * depth)
            entering[s, rows, :] = states[h]
            lane = s * 2 * heads + h
            decay = jnp.broadcast_to(columns[:, lane : lane + 1], (depth, 128))
            states[h] = decay * states[h] + received[s, rows, :].astype(F32)
    for h in range(heads):
        final[h] = states[h]
        final_out[h : h + 1, :] = final[h, pl.ds(lax.axis_index(Z), 1), :]
    mine = entering[lax.axis_index(Z)]
    for p in range(plane):
        send_out[p] = (prefix[p] + product[p] * mine).astype(BF16)

    @pl.when(jnp.logical_not(goes_early(depth)))
    def _():
        late_outputs(heads, query, value, gate, cumuls, keys, starts, offsets, gain,
                     raw_out, reach_out, gating_out)


def depth_scan(received, prefix, product, first, left, local, heads):
    depth, tall, _ = received.shape
    plane, rows, _ = prefix.shape
    return pl.pallas_call(
        functools.partial(depth_kernel, heads, plane, depth),
        in_specs=[VMEM_SPEC] * 15,
        out_specs=[VMEM_SPEC] * 5,
        out_shape=[
            jax.ShapeDtypeStruct((plane, rows, 128), BF16),
            jax.ShapeDtypeStruct((heads, 128), F32),
        ]
        + [jax.ShapeDtypeStruct(array.shape, array.dtype) for array in local],
        input_output_aliases={12: 2, 13: 3, 14: 4},
        scratch_shapes=[
            pltpu.VMEM((depth, rows, 128), F32),
            pltpu.VMEM((heads, depth, 128), F32),
        ],
        compiler_params=pltpu.CompilerParams(vmem_limit_bytes=30 * 1024 * 1024),
        cost_estimate=pl.CostEstimate(flops=100_000_000, bytes_accessed=1_000_000, transcendentals=0),
        name="depth_scan",
    )(received, prefix, product, first, *left, *local)


def gather_state(heads, depth, incoming, state):
    plane = incoming.shape[0]
    collect = deal_matrix(plane, depth, True)
    for h in range(heads):
        part = incoming[:, h * depth : (h + 1) * depth, :].astype(F32)
        part = part.reshape(plane * depth, 128).astype(BF16)
        state[h] = mm(collect, part).astype(BF16)


def gated_block(heads, source, raw, reach, gating, state, gated_out, target):
    rows = pl.ds(pl.multiple_of(source, BLOCK), BLOCK)
    for h in range(heads):
        cols = pl.ds(h * 128, 128)
        value = raw[rows, cols] + mm(reach[rows, cols], state[h])
        mean_square = jnp.mean(value * value, axis=-1, keepdims=True)
        gated_out[target : target + BLOCK, cols] = (
            value * lax.rsqrt(mean_square + EPSILON) * gating[rows, cols]
        ).astype(BF16)


def far_kernel(heads, depth, incoming, raw, reach, gating, gated_out, state):
    gather_state(heads, depth, incoming, state)
    half = gated_out.shape[0]
    first = (1 - lax.axis_index("tp")) * half
    for row in range(0, half, BLOCK):
        gated_block(heads, first + row, raw, reach, gating, state, gated_out, row)


def near_kernel(heads, tall, state, raw, reach, gating, weight, partial_out, gated):
    half = partial_out.shape[0]
    first = lax.axis_index("tp") * half
    for row in range(0, half, BLOCK):
        gated_block(heads, first + row, raw, reach, gating, state, gated, row)
        if (row + BLOCK) % tall == 0:
            done = pl.ds(row + BLOCK - tall, tall)
            partial_out[done, :] = mm(gated[done, :], weight[...])


def far_rows(incoming, raw, reach, gating, heads, depth):
    span, width = raw.shape
    return pl.pallas_call(
        functools.partial(far_kernel, heads, depth),
        in_specs=[VMEM_SPEC] * 4,
        out_specs=[VMEM_SPEC] * 2,
        out_shape=[
            jax.ShapeDtypeStruct((span // 2, width), BF16),
            jax.ShapeDtypeStruct((heads, 128, 128), BF16),
        ],
        compiler_params=pltpu.CompilerParams(vmem_limit_bytes=12 * 1024 * 1024),
        cost_estimate=pl.CostEstimate(flops=2_000_000_000, bytes_accessed=4_000_000, transcendentals=0),
        name="far_rows",
    )(incoming, raw, reach, gating)


def near_rows(state, raw, reach, gating, weight, heads, rows):
    span, width = raw.shape
    return pl.pallas_call(
        functools.partial(near_kernel, heads, rows),
        in_specs=[VMEM_SPEC] * 5,
        out_specs=VMEM_SPEC,
        out_shape=jax.ShapeDtypeStruct((span // 2, weight.shape[1]), F32),
        scratch_shapes=[pltpu.VMEM((span // 2, width), BF16)],
        compiler_params=pltpu.CompilerParams(vmem_limit_bytes=20 * 1024 * 1024),
        cost_estimate=pl.CostEstimate(flops=4_000_000_000, bytes_accessed=4_000_000, transcendentals=0),
        name="near_rows",
    )(state, raw, reach, gating, weight)


def project_kernel(partial, theirs, their_weight, final, out, final_out):
    out[...] = (partial[...] + mm(theirs[...], their_weight[...])).astype(BF16)
    final_out[...] = final[...]


def project(partial, theirs, their_weight, final, rows):
    total, width = partial.shape
    inner = theirs.shape[1]
    whole = pl.BlockSpec(final.shape, lambda i: (0, 0))
    return pl.pallas_call(
        project_kernel,
        grid=(total // rows,),
        in_specs=[
            pl.BlockSpec((rows, width), lambda i: (i, 0)),
            pl.BlockSpec((rows, inner), lambda i: (i, 0)),
            pl.BlockSpec((inner, width), lambda i: (0, 0)),
            whole,
        ],
        out_specs=[pl.BlockSpec((rows, width), lambda i: (i, 0)), whole],
        out_shape=[
            jax.ShapeDtypeStruct((total, width), BF16),
            jax.ShapeDtypeStruct(final.shape, F32),
        ],
        compiler_params=params(20),
        cost_estimate=pl.CostEstimate(flops=3_300_000_000, bytes_accessed=9_000_000, transcendentals=0),
        name="project",
    )(partial, theirs, pltpu.with_memory_space_constraint(their_weight, pltpu.VMEM), final)


def per_device(
    queries, forget_logit, value_rows, out_gate, floor_gap, head_gain, state_in, out_weight
):
    heads = state_in.shape[0]
    plane = lax.axis_size(PLANE)
    depth = lax.axis_size(Z)
    swap = [(0, 1), (1, 0)]
    barrier = lax.optimization_barrier
    gap = floor_gap.reshape(1, -1)
    gain = head_gain.reshape(1, -1)

    local, send, left = stretch(
        gap, gain, queries, forget_logit, value_rows, out_gate, heads, plane, depth, UNROLL
    )
    send, out_weight = barrier((send, out_weight))
    their_weight = lax.ppermute(out_weight, "tp", swap)
    received = lax.all_to_all(send, PLANE, 0, 0, tiled=True)

    send, prefix, product = plane_scan(received, heads, depth)
    received = lax.all_to_all(send, Z, 0, 0, tiled=True)
    send, final, *local = depth_scan(
        received, prefix, product, state_in, left, local, heads
    )
    incoming = lax.all_to_all(send, PLANE, 0, 0, tiled=True)

    far, state = far_rows(incoming, *local, heads, depth)
    theirs = lax.ppermute(far, "tp", swap)
    partial = near_rows(state, *local, out_weight, heads, 384)
    projected, state_out = project(partial, theirs, their_weight, final, 384)
    return (projected, state_out)


def solution(mesh):
    torus = Mesh(mesh.devices.reshape(8, 4, 4, mesh.shape["tp"]), (Z, Y, X, "tp"))
    placed = (
        P(SP, "tp"),
        P(SP, "tp"),
        P(SP, "tp"),
        P(SP, "tp"),
        P("tp"),
        P("tp"),
        P("tp", None, None),
        P("tp", None),
    )
    return jax.shard_map(
        per_device,
        mesh=torus,
        in_specs=placed,
        out_specs=(P(SP_TP, None), P("tp", SP)),
        check_vma=False,
    )
```

time: 62.3 us -> 57.9 us (0.929)
  blocking collectives: 37.1 us -> 34.5 us
  Pallas kernels: 16.7 us -> 15 us
    all_to_all x1, blocking collectives: 15.4 us -> 12.8 us  [per_device(): received = lax.all_to_all(send, Z, 0, 0, tiled=True)]
  transfers between devices with their start and end apart: 2 -> 2, of which waited for: 0 -> 0; matrix products, arithmetic and copies ran while one was open for 0% -> 0% of each run, Pallas kernels for 9% -> 7%
where the time goes in v4:
time: 57.9 us; the launch traced here: 57.8 us
  blocking collectives  34.5 us (60%)
  Pallas kernels  15 us (26%)
  starting transfers between devices  7.51 us (13%)
  between operations  0.71 us (1%)
    all_to_all x1, blocking collectives, per_device(): received = lax.all_to_all(send, Z, 0, 0, tiled=True)  12.8 us
    all_to_all x1, blocking collectives, per_device(): received = lax.all_to_all(send, PLANE, 0, 0, tiled=True)  12.3 us
    all_to_all x1, blocking collectives, per_device(): incoming = lax.all_to_all(send, PLANE, 0, 0, tiled=True)  9.48 us
    pallas_call x1, Pallas kernels, stretch(): pl.pallas_call(functools.partial(stretch_kernel, heads, plane, depth, unr...  7.56 us
    ppermute x1, starting transfers between devices, per_device(): theirs = lax.ppermute(far, 'tp', swap)  4.22 us
    ppermute x1, starting transfers between devices, per_device(): their_weight = lax.ppermute(out_weight, 'tp', swap)  3.29 us
    pallas_call x1, Pallas kernels, project(): pl.pallas_call(project_kernel, grid=(total // rows,), in_specs=[pl.BlockS...  3.21 us
    pallas_call x1, Pallas kernels, near_rows(): pl.pallas_call(functools.partial(near_kernel, heads, rows), in_specs=[VME...  2.45 us
  transfers between devices with their start and end apart: 2, of which 0 were waited for; matrix products, arithmetic and copies ran while one was open for 0% of the time, Pallas kernels for 7%

profile of v4, /device:TPU:1, one launch (start us, length us, event | category | flops | bytes accessed | tf_op | source)
XLA Modules:
  0.0 57.8 jit_solution(955078178352189642)
XLA Ops:
  0.6 0.0 copy-start
  0.6 0.0 copy-start.1
  0.7 7.6 %stretch.1 = (f32[1536,512]{1,0:T(8,128)S(1)}, bf16[1536,512]{1,0:T(8,128)(2,1)S(1)}, f32[1536,512]{1,0:T(8,128)S(1)}, bf16[16,40,128]{2,1,0:T(8,128)(2,1)S(1)},...) custom-call(f32[1,512]{1,0:T(1,128)} %bitcast.2, ...), custom_call_target="tpu_custom_call" | custom-call | flops 6000000000 | bytes 10000000 | tf_op jit(solution)/shard_map/stretch/pallas_call | solution.py:220
  8.2 0.0 copy-done
  8.2 3.3 %collective-permute-start.1 = (bf16[512,2048]{1,0:T(8,128)(2,1)S(1)}, bf16[512,2048]{1,0:T(8,128)(2,1)S(1)}, u32[]{:S(2)}, u32[]{:S(2)}) collective-permute-start(bf16[512,2048]{1,0:T(8,128)(2,1)S(1)} %copy-done), channel_id=1, source_target_pairs={{0,1},{1,0},{2,3},{3,2},{4,5},{5,4},{6,7},{7,6},{8,9},{9,8},{10,11... | collective-permute-start | bytes 6291464 | tf_op jit(solution)/shard_map/ppermute | solution.py:467
  11.5 12.3 %all_to_all.15.received = bf16[16,40,128]{2,1,0:T(8,128)(2,1)S(1)} all-to-all(bf16[16,40,128]{2,1,0:T(8,128)(2,1)S(1)} %get-tuple-element.27), channel_id=1, replica_groups=mesh['sp_0'=8,'sp_1'=4,'sp_2'=4,'tp'=2] {'sp_1','sp_2'}, dimensions={0} | all-to-all | bytes 327680 | tf_op jit(solution)/shard_map/all_to_all | solution.py:468
  23.8 0.4 plane_scan.1
  24.2 12.8 %all_to_all.16.received = bf16[8,40,128]{2,1,0:T(8,128)(2,1)S(1)} all-to-all(bf16[8,40,128]{2,1,0:T(8,128)(2,1)S(1)} %get-tuple-element.28), channel_id=1, replica_groups=mesh['sp_0'=8,'sp_1'=4,'sp_2'=4,'tp'=2] {'sp_0'}, dimensions={0} | all-to-all | bytes 163840 | tf_op jit(solution)/shard_map/all_to_all | solution.py:471
  37.0 0.0 copy-done.1
  37.0 0.5 depth_scan.1
  37.5 9.5 %all_to_all.17.incoming = bf16[16,32,128]{2,1,0:T(8,128)(2,1)S(1)} all-to-all(bf16[16,32,128]{2,1,0:T(8,128)(2,1)S(1)} %get-tuple-element.42), channel_id=1, replica_groups=mesh['sp_0'=8,'sp_1'=4,'sp_2'=4,'tp'=2] {'sp_1','sp_2'}, dimensions={0} | all-to-all | bytes 262144 | tf_op jit(solution)/shard_map/all_to_all | solution.py:475
  47.0 0.9 %far_rows.1 = (bf16[768,512]{1,0:T(8,128)(2,1)S(1)}, bf16[4,128,128]{2,1,0:T(8,128)(2,1)S(1)}) custom-call(bf16[16,32,128]{2,1,0:T(8,128)(2,1)S(1)} %all_to_all.17.incoming, f32[1536,512]{1,0:T(8,128)S(1)} %get-tuple-element.43.raw, bf16[1536,512]{1,0:T(8,128)(2,1)S(1)} %get-tuple-element.44.reach, f32[1536,512]{1,0:T(8,128)S(1)} %get-tuple-element.45.gating), custom_call_target="tpu_custom_call" | custom-call | flops 2000000000 | bytes 4000000 | tf_op jit(solution)/shard_map/far_rows/pallas_call | solution.py:395
  47.8 4.2 %collective-permute-start = (bf16[768,512]{1,0:T(8,128)(2,1)S(1)}, bf16[768,512]{1,0:T(8,128)(2,1)S(1)}, u32[]{:S(2)}, u32[]{:S(2)}) collective-permute-start(bf16[768,512]{1,0:T(8,128)(2,1)S(1)} %get-tuple-element.48), channel_id=1, source_target_pairs={{0,1},{1,0},{2,3},{3,2},{4,5},{5,4},{6,7},{7,6},{8,9},{9,8},{10,11... | collective-permute-start | bytes 2359304 | tf_op jit(solution)/shard_map/ppermute | solution.py:478
  52.1 2.5 %near_rows.1.partial = f32[768,2048]{1,0:T(8,128)S(1)} custom-call(bf16[4,128,128]{2,1,0:T(8,128)(2,1)S(1)} %get-tuple-element.46.state, f32[1536,512]{1,0:T(8,128)S(1)} %get-tuple-element.43.raw, bf16[1536,512]{1,0:T(8,128)(2,1)S(1)} %get-tuple-element.44.reach, f32[1536,512]{1,0:T(8,128)S(1)} %get-tuple-element.45.gating, bf16[512,2048]{1,0:T(8,128)(2,1)S(1)} %copy-done), custom_call_target="tpu_custom_call" | custom-call | flops 4000000000 | bytes 4000000 | tf_op jit(solution)/shard_map/near_rows/pallas_call | solution.py:411
  54.5 0.0 collective-permute-done.theirs
  54.5 0.0 collective-permute-done.1.their_weight
  54.5 3.2 %project.1 = (bf16[768,2048]{1,0:T(8,128)(2,1)}, f32[4,128]{1,0:T(4,128)}) custom-call(f32[768,2048]{1,0:T(8,128)S(1)} %near_rows.1.partial, bf16[768,512]{1,0:T(8,128)(2,1)S(1)} %collective-permute-done.theirs, bf16[512,2048]{1,0:T(8,128)(2,1)S(1)} %collective-permute-done.1.their_weight, f32[4,128]{1,0:T(4,128)S(1)} %get-tuple-element.49.final), custom_call_target="tpu_custom_call" | custom-call | flops 3300000000 | bytes 9000000 | tf_op jit(solution)/shard_map/project/pallas_call | solution.py:432
Async XLA Ops:
  0.6 7.6 %copy-start = (bf16[512,2048]{1,0:T(8,128)(2,1)S(1)}, bf16[512,2048]{1,0:T(8,128)(2,1)}, u32[]{:S(2)}) copy-start(bf16[512,2048]{1,0:T(8,128)(2,1)} %weight) | copy-start | bytes 6291460
  0.6 36.3 %copy-start.1 = (f32[4,128,128]{2,1,0:T(8,128)S(1)}, f32[4,128,128]{2,1,0:T(8,128)}, u32[]{:S(2)}) copy-start(f32[4,128,128]{2,1,0:T(8,128)} %first.1) | copy-start | bytes 786436
  8.2 46.3 %collective-permute-start.1 = (bf16[512,2048]{1,0:T(8,128)(2,1)S(1)}, bf16[512,2048]{1,0:T(8,128)(2,1)S(1)}, u32[]{:S(2)}, u32[]{:S(2)}) collective-permute-start(bf16[512,2048]{1,0:T(8,128)(2,1)S(1)} %copy-done), channel_id=1, source_target_pairs={{0,1},{1,0},{2,3},{3,2},{4,5},{5,4},{6,7},{7,6},{8,9},{9,8},{10,11... | collective-permute-start | bytes 6291464 | tf_op jit(solution)/shard_map/ppermute | solution.py:467
  47.8 6.7 %collective-permute-start = (bf16[768,512]{1,0:T(8,128)(2,1)S(1)}, bf16[768,512]{1,0:T(8,128)(2,1)S(1)}, u32[]{:S(2)}, u32[]{:S(2)}) collective-permute-start(bf16[768,512]{1,0:T(8,128)(2,1)S(1)} %get-tuple-element.48), channel_id=1, source_target_pairs={{0,1},{1,0},{2,3},{3,2},{4,5},{5,4},{6,7},{7,6},{8,9},{9,8},{10,11... | collective-permute-start | bytes 2359304 | tf_op jit(solution)/shard_map/ppermute | solution.py:478

commit v5 on v4

--- a/solution.py
+++ b/solution.py
@@ -86,9 +86,10 @@
         pltpu.make_async_copy(gap_in, gap, small_sems.at[0]),
         pltpu.make_async_copy(gain_in, gain, small_sems.at[1]),
     ]
+    logits(0).start()
     for copy in small:
         copy.start()
-    for i in range(blocks // unroll):
+    for i in range(1, blocks // unroll):
         logits(i).start()
     for copy in rest:
         copy.start()
@@ -476,7 +477,7 @@
 
     far, state = far_rows(incoming, *local, heads, depth)
     theirs = lax.ppermute(far, "tp", swap)
-    partial = near_rows(state, *local, out_weight, heads, 384)
+    partial = near_rows(state, *local, out_weight, heads, 768)
     projected, state_out = project(partial, theirs, their_weight, final, 384)
     return (projected, state_out)
 

time: 57.9 us -> 57.7 us (level)
  no operation moved by 1% of the time
where the time goes in v5:
time: 57.7 us; the launch traced here: 57.5 us
  blocking collectives  34.5 us (60%)
  Pallas kernels  14.8 us (26%)
  starting transfers between devices  7.51 us (13%)
  between operations  0.71 us (1%)
    all_to_all x1, blocking collectives, per_device(): received = lax.all_to_all(send, Z, 0, 0, tiled=True)  12.8 us
    all_to_all x1, blocking collectives, per_device(): received = lax.all_to_all(send, PLANE, 0, 0, tiled=True)  12.3 us
    all_to_all x1, blocking collectives, per_device(): incoming = lax.all_to_all(send, PLANE, 0, 0, tiled=True)  9.48 us
    pallas_call x1, Pallas kernels, stretch(): pl.pallas_call(functools.partial(stretch_kernel, heads, plane, depth, unr...  7.55 us
    ppermute x1, starting transfers between devices, per_device(): theirs = lax.ppermute(far, 'tp', swap)  4.22 us
    ppermute x1, starting transfers between devices, per_device(): their_weight = lax.ppermute(out_weight, 'tp', swap)  3.29 us
    pallas_call x1, Pallas kernels, project(): pl.pallas_call(project_kernel, grid=(total // rows,), in_specs=[pl.BlockS...  3.21 us
    pallas_call x1, Pallas kernels, near_rows(): pl.pallas_call(functools.partial(near_kernel, heads, rows), in_specs=[VME...  2.24 us
  transfers between devices with their start and end apart: 2, of which 0 were waited for; matrix products, arithmetic and copies ran while one was open for 0% of the time, Pallas kernels for 7%

profile of v5, /device:TPU:1, one launch (start us, length us, event | category | flops | bytes accessed | tf_op | source)
XLA Modules:
  0.0 57.5 jit_solution(13183133680062579156)
XLA Ops:
  0.6 0.0 copy-start
  0.6 0.0 copy-start.1
  0.7 7.6 %stretch.1 = (f32[1536,512]{1,0:T(8,128)S(1)}, bf16[1536,512]{1,0:T(8,128)(2,1)S(1)}, f32[1536,512]{1,0:T(8,128)S(1)}, bf16[16,40,128]{2,1,0:T(8,128)(2,1)S(1)},...) custom-call(f32[1,512]{1,0:T(1,128)} %bitcast.2, ...), custom_call_target="tpu_custom_call" | custom-call | flops 6000000000 | bytes 10000000 | tf_op jit(solution)/shard_map/stretch/pallas_call | solution.py:221
  8.2 0.0 copy-done
  8.2 3.3 %collective-permute-start.1 = (bf16[512,2048]{1,0:T(8,128)(2,1)S(1)}, bf16[512,2048]{1,0:T(8,128)(2,1)S(1)}, u32[]{:S(2)}, u32[]{:S(2)}) collective-permute-start(bf16[512,2048]{1,0:T(8,128)(2,1)S(1)} %copy-done), channel_id=1, source_target_pairs={{0,1},{1,0},{2,3},{3,2},{4,5},{5,4},{6,7},{7,6},{8,9},{9,8},{10,11... | collective-permute-start | bytes 6291464 | tf_op jit(solution)/shard_map/ppermute | solution.py:468
  11.5 12.3 %all_to_all.15.received = bf16[16,40,128]{2,1,0:T(8,128)(2,1)S(1)} all-to-all(bf16[16,40,128]{2,1,0:T(8,128)(2,1)S(1)} %get-tuple-element.27), channel_id=1, replica_groups=mesh['sp_0'=8,'sp_1'=4,'sp_2'=4,'tp'=2] {'sp_1','sp_2'}, dimensions={0} | all-to-all | bytes 327680 | tf_op jit(solution)/shard_map/all_to_all | solution.py:469
  23.8 0.4 plane_scan.1
  24.2 12.8 %all_to_all.16.received = bf16[8,40,128]{2,1,0:T(8,128)(2,1)S(1)} all-to-all(bf16[8,40,128]{2,1,0:T(8,128)(2,1)S(1)} %get-tuple-element.28), channel_id=1, replica_groups=mesh['sp_0'=8,'sp_1'=4,'sp_2'=4,'tp'=2] {'sp_0'}, dimensions={0} | all-to-all | bytes 163840 | tf_op jit(solution)/shard_map/all_to_all | solution.py:472
  37.0 0.0 copy-done.1
  37.0 0.5 depth_scan.1
  37.5 9.5 %all_to_all.17.incoming = bf16[16,32,128]{2,1,0:T(8,128)(2,1)S(1)} all-to-all(bf16[16,32,128]{2,1,0:T(8,128)(2,1)S(1)} %get-tuple-element.42), channel_id=1, replica_groups=mesh['sp_0'=8,'sp_1'=4,'sp_2'=4,'tp'=2] {'sp_1','sp_2'}, dimensions={0} | all-to-all | bytes 262144 | tf_op jit(solution)/shard_map/all_to_all | solution.py:476
  47.0 0.9 %far_rows.1 = (bf16[768,512]{1,0:T(8,128)(2,1)S(1)}, bf16[4,128,128]{2,1,0:T(8,128)(2,1)S(1)}) custom-call(bf16[16,32,128]{2,1,0:T(8,128)(2,1)S(1)} %all_to_all.17.incoming, f32[1536,512]{1,0:T(8,128)S(1)} %get-tuple-element.43.raw, bf16[1536,512]{1,0:T(8,128)(2,1)S(1)} %get-tuple-element.44.reach, f32[1536,512]{1,0:T(8,128)S(1)} %get-tuple-element.45.gating), custom_call_target="tpu_custom_call" | custom-call | flops 2000000000 | bytes 4000000 | tf_op jit(solution)/shard_map/far_rows/pallas_call | solution.py:396
  47.8 4.2 %collective-permute-start = (bf16[768,512]{1,0:T(8,128)(2,1)S(1)}, bf16[768,512]{1,0:T(8,128)(2,1)S(1)}, u32[]{:S(2)}, u32[]{:S(2)}) collective-permute-start(bf16[768,512]{1,0:T(8,128)(2,1)S(1)} %get-tuple-element.48), channel_id=1, source_target_pairs={{0,1},{1,0},{2,3},{3,2},{4,5},{5,4},{6,7},{7,6},{8,9},{9,8},{10,11... | collective-permute-start | bytes 2359304 | tf_op jit(solution)/shard_map/ppermute | solution.py:479
  52.1 2.2 %near_rows.1.partial = f32[768,2048]{1,0:T(8,128)S(1)} custom-call(bf16[4,128,128]{2,1,0:T(8,128)(2,1)S(1)} %get-tuple-element.46.state, f32[1536,512]{1,0:T(8,128)S(1)} %get-tuple-element.43.raw, bf16[1536,512]{1,0:T(8,128)(2,1)S(1)} %get-tuple-element.44.reach, f32[1536,512]{1,0:T(8,128)S(1)} %get-tuple-element.45.gating, bf16[512,2048]{1,0:T(8,128)(2,1)S(1)} %copy-done), custom_call_target="tpu_custom_call" | custom-call | flops 4000000000 | bytes 4000000 | tf_op jit(solution)/shard_map/near_rows/pallas_call | solution.py:412
  54.3 0.0 collective-permute-done.theirs
  54.3 0.0 collective-permute-done.1.their_weight
  54.3 3.2 %project.1 = (bf16[768,2048]{1,0:T(8,128)(2,1)}, f32[4,128]{1,0:T(4,128)}) custom-call(f32[768,2048]{1,0:T(8,128)S(1)} %near_rows.1.partial, bf16[768,512]{1,0:T(8,128)(2,1)S(1)} %collective-permute-done.theirs, bf16[512,2048]{1,0:T(8,128)(2,1)S(1)} %collective-permute-done.1.their_weight, f32[4,128]{1,0:T(4,128)S(1)} %get-tuple-element.49.final), custom_call_target="tpu_custom_call" | custom-call | flops 3300000000 | bytes 9000000 | tf_op jit(solution)/shard_map/project/pallas_call | solution.py:433
Async XLA Ops:
  0.6 7.6 %copy-start = (bf16[512,2048]{1,0:T(8,128)(2,1)S(1)}, bf16[512,2048]{1,0:T(8,128)(2,1)}, u32[]{:S(2)}) copy-start(bf16[512,2048]{1,0:T(8,128)(2,1)} %weight) | copy-start | bytes 6291460
  0.6 36.3 %copy-start.1 = (f32[4,128,128]{2,1,0:T(8,128)S(1)}, f32[4,128,128]{2,1,0:T(8,128)}, u32[]{:S(2)}) copy-start(f32[4,128,128]{2,1,0:T(8,128)} %first.1) | copy-start | bytes 786436
  8.2 46.1 %collective-permute-start.1 = (bf16[512,2048]{1,0:T(8,128)(2,1)S(1)}, bf16[512,2048]{1,0:T(8,128)(2,1)S(1)}, u32[]{:S(2)}, u32[]{:S(2)}) collective-permute-start(bf16[512,2048]{1,0:T(8,128)(2,1)S(1)} %copy-done), channel_id=1, source_target_pairs={{0,1},{1,0},{2,3},{3,2},{4,5},{5,4},{6,7},{7,6},{8,9},{9,8},{10,11... | collective-permute-start | bytes 6291464 | tf_op jit(solution)/shard_map/ppermute | solution.py:468
  47.8 6.5 %collective-permute-start = (bf16[768,512]{1,0:T(8,128)(2,1)S(1)}, bf16[768,512]{1,0:T(8,128)(2,1)S(1)}, u32[]{:S(2)}, u32[]{:S(2)}) collective-permute-start(bf16[768,512]{1,0:T(8,128)(2,1)S(1)} %get-tuple-element.48), channel_id=1, source_target_pairs={{0,1},{1,0},{2,3},{3,2},{4,5},{5,4},{6,7},{7,6},{8,9},{9,8},{10,11... | collective-permute-start | bytes 2359304 | tf_op jit(solution)/shard_map/ppermute | solution.py:479

commit v6 on v5

--- a/solution.py
+++ b/solution.py
@@ -47,7 +47,7 @@
 
 
 def goes_early(depth):
-    return lax.axis_index(Z) < depth * 3 // 8
+    return lax.axis_index(Z) < depth // 4
 
 
 def rows_of(block):

time: 57.7 us -> 57.7 us (level)
  no operation moved by 1% of the time
where the time goes in v6:
time: 57.7 us; the launch traced here: 57.5 us
  blocking collectives  34.5 us (60%)
  Pallas kernels  14.8 us (26%)
  starting transfers between devices  7.51 us (13%)
  between operations  0.71 us (1%)
    all_to_all x1, blocking collectives, per_device(): received = lax.all_to_all(send, Z, 0, 0, tiled=True)  12.8 us
    all_to_all x1, blocking collectives, per_device(): received = lax.all_to_all(send, PLANE, 0, 0, tiled=True)  12.3 us
    all_to_all x1, blocking collectives, per_device(): incoming = lax.all_to_all(send, PLANE, 0, 0, tiled=True)  9.48 us
    pallas_call x1, Pallas kernels, stretch(): pl.pallas_call(functools.partial(stretch_kernel, heads, plane, depth, unr...  7.55 us
    ppermute x1, starting transfers between devices, per_device(): theirs = lax.ppermute(far, 'tp', swap)  4.22 us
    ppermute x1, starting transfers between devices, per_device(): their_weight = lax.ppermute(out_weight, 'tp', swap)  3.29 us
    pallas_call x1, Pallas kernels, project(): pl.pallas_call(project_kernel, grid=(total // rows,), in_specs=[pl.BlockS...  3.21 us
    pallas_call x1, Pallas kernels, near_rows(): pl.pallas_call(functools.partial(near_kernel, heads, rows), in_specs=[VME...  2.24 us
  transfers between devices with their start and end apart: 2, of which 0 were waited for; matrix products, arithmetic and copies ran while one was open for 0% of the time, Pallas kernels for 7%

profile of v6, /device:TPU:1, one launch (start us, length us, event | category | flops | bytes accessed | tf_op | source)
XLA Modules:
  0.0 57.5 jit_solution(1752418817578730462)
XLA Ops:
  0.6 0.0 copy-start
  0.6 0.0 copy-start.1
  0.7 7.6 %stretch.1 = (f32[1536,512]{1,0:T(8,128)S(1)}, bf16[1536,512]{1,0:T(8,128)(2,1)S(1)}, f32[1536,512]{1,0:T(8,128)S(1)}, bf16[16,40,128]{2,1,0:T(8,128)(2,1)S(1)},...) custom-call(f32[1,512]{1,0:T(1,128)} %bitcast.2, ...), custom_call_target="tpu_custom_call" | custom-call | flops 6000000000 | bytes 10000000 | tf_op jit(solution)/shard_map/stretch/pallas_call | solution.py:221
  8.2 0.0 copy-done
  8.2 3.3 %collective-permute-start.1 = (bf16[512,2048]{1,0:T(8,128)(2,1)S(1)}, bf16[512,2048]{1,0:T(8,128)(2,1)S(1)}, u32[]{:S(2)}, u32[]{:S(2)}) collective-permute-start(bf16[512,2048]{1,0:T(8,128)(2,1)S(1)} %copy-done), channel_id=1, source_target_pairs={{0,1},{1,0},{2,3},{3,2},{4,5},{5,4},{6,7},{7,6},{8,9},{9,8},{10,11... | collective-permute-start | bytes 6291464 | tf_op jit(solution)/shard_map/ppermute | solution.py:468
  11.5 12.3 %all_to_all.15.received = bf16[16,40,128]{2,1,0:T(8,128)(2,1)S(1)} all-to-all(bf16[16,40,128]{2,1,0:T(8,128)(2,1)S(1)} %get-tuple-element.27), channel_id=1, replica_groups=mesh['sp_0'=8,'sp_1'=4,'sp_2'=4,'tp'=2] {'sp_1','sp_2'}, dimensions={0} | all-to-all | bytes 327680 | tf_op jit(solution)/shard_map/all_to_all | solution.py:469
  23.8 0.4 plane_scan.1
  24.2 12.8 %all_to_all.16.received = bf16[8,40,128]{2,1,0:T(8,128)(2,1)S(1)} all-to-all(bf16[8,40,128]{2,1,0:T(8,128)(2,1)S(1)} %get-tuple-element.28), channel_id=1, replica_groups=mesh['sp_0'=8,'sp_1'=4,'sp_2'=4,'tp'=2] {'sp_0'}, dimensions={0} | all-to-all | bytes 163840 | tf_op jit(solution)/shard_map/all_to_all | solution.py:472
  37.0 0.0 copy-done.1
  37.0 0.5 depth_scan.1
  37.5 9.5 %all_to_all.17.incoming = bf16[16,32,128]{2,1,0:T(8,128)(2,1)S(1)} all-to-all(bf16[16,32,128]{2,1,0:T(8,128)(2,1)S(1)} %get-tuple-element.42), channel_id=1, replica_groups=mesh['sp_0'=8,'sp_1'=4,'sp_2'=4,'tp'=2] {'sp_1','sp_2'}, dimensions={0} | all-to-all | bytes 262144 | tf_op jit(solution)/shard_map/all_to_all | solution.py:476
  47.0 0.9 %far_rows.1 = (bf16[768,512]{1,0:T(8,128)(2,1)S(1)}, bf16[4,128,128]{2,1,0:T(8,128)(2,1)S(1)}) custom-call(bf16[16,32,128]{2,1,0:T(8,128)(2,1)S(1)} %all_to_all.17.incoming, f32[1536,512]{1,0:T(8,128)S(1)} %get-tuple-element.43.raw, bf16[1536,512]{1,0:T(8,128)(2,1)S(1)} %get-tuple-element.44.reach, f32[1536,512]{1,0:T(8,128)S(1)} %get-tuple-element.45.gating), custom_call_target="tpu_custom_call" | custom-call | flops 2000000000 | bytes 4000000 | tf_op jit(solution)/shard_map/far_rows/pallas_call | solution.py:396
  47.8 4.2 %collective-permute-start = (bf16[768,512]{1,0:T(8,128)(2,1)S(1)}, bf16[768,512]{1,0:T(8,128)(2,1)S(1)}, u32[]{:S(2)}, u32[]{:S(2)}) collective-permute-start(bf16[768,512]{1,0:T(8,128)(2,1)S(1)} %get-tuple-element.48), channel_id=1, source_target_pairs={{0,1},{1,0},{2,3},{3,2},{4,5},{5,4},{6,7},{7,6},{8,9},{9,8},{10,11... | collective-permute-start | bytes 2359304 | tf_op jit(solution)/shard_map/ppermute | solution.py:479
  52.1 2.2 %near_rows.1.partial = f32[768,2048]{1,0:T(8,128)S(1)} custom-call(bf16[4,128,128]{2,1,0:T(8,128)(2,1)S(1)} %get-tuple-element.46.state, f32[1536,512]{1,0:T(8,128)S(1)} %get-tuple-element.43.raw, bf16[1536,512]{1,0:T(8,128)(2,1)S(1)} %get-tuple-element.44.reach, f32[1536,512]{1,0:T(8,128)S(1)} %get-tuple-element.45.gating, bf16[512,2048]{1,0:T(8,128)(2,1)S(1)} %copy-done), custom_call_target="tpu_custom_call" | custom-call | flops 4000000000 | bytes 4000000 | tf_op jit(solution)/shard_map/near_rows/pallas_call | solution.py:412
  54.3 0.0 collective-permute-done.theirs
  54.3 0.0 collective-permute-done.1.their_weight
  54.3 3.2 %project.1 = (bf16[768,2048]{1,0:T(8,128)(2,1)}, f32[4,128]{1,0:T(4,128)}) custom-call(f32[768,2048]{1,0:T(8,128)S(1)} %near_rows.1.partial, bf16[768,512]{1,0:T(8,128)(2,1)S(1)} %collective-permute-done.theirs, bf16[512,2048]{1,0:T(8,128)(2,1)S(1)} %collective-permute-done.1.their_weight, f32[4,128]{1,0:T(4,128)S(1)} %get-tuple-element.49.final), custom_call_target="tpu_custom_call" | custom-call | flops 3300000000 | bytes 9000000 | tf_op jit(solution)/shard_map/project/pallas_call | solution.py:433
Async XLA Ops:
  0.6 7.6 %copy-start = (bf16[512,2048]{1,0:T(8,128)(2,1)S(1)}, bf16[512,2048]{1,0:T(8,128)(2,1)}, u32[]{:S(2)}) copy-start(bf16[512,2048]{1,0:T(8,128)(2,1)} %weight) | copy-start | bytes 6291460
  0.6 36.3 %copy-start.1 = (f32[4,128,128]{2,1,0:T(8,128)S(1)}, f32[4,128,128]{2,1,0:T(8,128)}, u32[]{:S(2)}) copy-start(f32[4,128,128]{2,1,0:T(8,128)} %first.1) | copy-start | bytes 786436
  8.2 46.1 %collective-permute-start.1 = (bf16[512,2048]{1,0:T(8,128)(2,1)S(1)}, bf16[512,2048]{1,0:T(8,128)(2,1)S(1)}, u32[]{:S(2)}, u32[]{:S(2)}) collective-permute-start(bf16[512,2048]{1,0:T(8,128)(2,1)S(1)} %copy-done), channel_id=1, source_target_pairs={{0,1},{1,0},{2,3},{3,2},{4,5},{5,4},{6,7},{7,6},{8,9},{9,8},{10,11... | collective-permute-start | bytes 6291464 | tf_op jit(solution)/shard_map/ppermute | solution.py:468
  47.8 6.5 %collective-permute-start = (bf16[768,512]{1,0:T(8,128)(2,1)S(1)}, bf16[768,512]{1,0:T(8,128)(2,1)S(1)}, u32[]{:S(2)}, u32[]{:S(2)}) collective-permute-start(bf16[768,512]{1,0:T(8,128)(2,1)S(1)} %get-tuple-element.48), channel_id=1, source_target_pairs={{0,1},{1,0},{2,3},{3,2},{4,5},{5,4},{6,7},{7,6},{8,9},{9,8},{10,11... | collective-permute-start | bytes 2359304 | tf_op jit(solution)/shard_map/ppermute | solution.py:479
